TPU v7x, 32 devices: a whole 2x2x4 slice. The times are simulated.
32 devices in a mesh: fs: 8 (over z, y), tp: 4 (over x, core).
Axes of the slice: x: 2, y: 2, z: 4, core: 2. Of those that a mesh axis runs over, the one named last changes fastest.
Arguments:
- inputs: bfloat16 [4096, 2112], P('fs', 'tp'), may hold values from -6 to 6
- w_conv_up: bfloat16 [2112, 2816], P('fs', 'tp'), may hold values from -0.125 to 0.125
- w_gate_up: bfloat16 [2112, 2816], P('fs', 'tp'), may hold values from -0.125 to 0.125
- w_down: bfloat16 [2816, 2112], P('tp', 'fs'), may hold values from -0.109375 to 0.109375
- taps: float32 [3, 2816], replicated, may hold values from -3 to 3
- conv_bias: float32 [2816], replicated, may hold values from -3 to 3
- cotangent: bfloat16 [4096, 2112], P('fs', 'tp'), may hold values from -6 to 6
Outputs:
- grad_inputs: bfloat16 [4096, 2112], P('fs', 'tp')
- grad_conv_up: float32 [2112, 2816], P('fs', 'tp')
- unit_norms: float32 [2816], P('tp')
- grad_taps: float32 [3, 2816], replicated
- grad_bias: float32 [2816], replicated
All inputs are finite; a program needn't handle non-finite values.
Results may differ from a plain program's by a relative error of at most 0.018.
Values may be sent and summed in bfloat16 or wider, within the bound.
A program may use at most 64 MiB of HBM per device.

v0:
```python
import functools
import math

import jax
import jax.numpy as jnp
from jax import lax
from jax.experimental import pallas as pl
from jax.experimental.pallas import tpu as pltpu
from jax.sharding import PartitionSpec as P

TAPS = 3
LANES = 128
MESH = pl.DeviceIdType.MESH
VMEM = pl.BlockSpec(memory_space=pltpu.VMEM)
ANY = pl.BlockSpec(memory_space=pl.ANY)


def shifted(block, axis, distance):
    devices = range(lax.axis_size(axis))
    route = [(i - distance, i) for i in devices if i - distance in devices]
    return lax.ppermute(block, axis, route)


def gelu_parts(value):
    normal_cdf = 0.5 * (1.0 + jax.scipy.special.erf(value / math.sqrt(2.0)))
    density = jnp.exp(-0.5 * value * value) / math.sqrt(2.0 * math.pi)
    return (value * normal_cdf, normal_cdf + value * density)


def with_collectives(inputs, w_conv_up, w_gate_up, w_down, taps, conv_bias, cotangent):
    span = TAPS - 1
    rows = inputs.shape[0]
    width = w_conv_up.shape[1]
    col_start = lax.axis_index("tp") * width
    taps_own = lax.dynamic_slice_in_dim(taps, col_start, width, 1)
    bias_own = lax.dynamic_slice_in_dim(conv_bias, col_start, width, 0)
    features, cot_full = (
        lax.all_gather(inputs, "tp", axis=1, tiled=True),
        lax.all_gather(cotangent, "tp", axis=1, tiled=True),
    )
    conv_weight, gate_weight = (
        lax.all_gather(w_conv_up, "fs", axis=0, tiled=True),
        lax.all_gather(w_gate_up, "fs", axis=0, tiled=True),
    )
    columns = cot_full
    d_hidden = lax.dot_general(
        columns,
        lax.all_gather(w_down, "fs", axis=1, tiled=True),
        (((1,), (1,)), ((), ())),
        preferred_element_type=jnp.float32,
    ).astype(jnp.bfloat16)
    up_a = jnp.dot(features, conv_weight, preferred_element_type=jnp.float32).astype(jnp.bfloat16)
    up_b = jnp.dot(features, gate_weight, preferred_element_type=jnp.float32).astype(jnp.bfloat16)
    earlier = shifted(up_a[rows - span :], "fs", 1)
    extended = jnp.concatenate([earlier, up_a], 0).astype(jnp.float32)
    conv_out = bias_own[None, :] + sum(
        (taps_own[i][None, :] * extended[i : i + rows] for i in range(TAPS))
    )
    gelu_value, gelu_slope = gelu_parts(conv_out)
    hidden_grad = d_hidden.astype(jnp.float32)
    d_conv = hidden_grad * up_b.astype(jnp.float32) * gelu_slope
    d_up_b = (hidden_grad * gelu_value).astype(jnp.bfloat16)
    later = shifted(d_conv[:span], "fs", -1)
    d_extended = jnp.concatenate([d_conv, later], 0)
    d_up_a = sum(
        (taps_own[i][None, :] * d_extended[span - i : span - i + rows] for i in range(TAPS))
    ).astype(jnp.bfloat16)
    tap_terms = [jnp.sum(d_conv * extended[i : i + rows], axis=0) for i in range(TAPS)]
    column_part = jnp.stack(tap_terms + [jnp.sum(d_conv, axis=0)], 0)
    contract = (((1,), (1,)), ((), ()))
    partial_sum = lax.dot_general(d_up_a, conv_weight, contract, preferred_element_type=jnp.float32)
    partial_sum = partial_sum + lax.dot_general(
        d_up_b, gate_weight, contract, preferred_element_type=jnp.float32
    )
    grad_inputs = lax.psum_scatter(
        partial_sum.astype(jnp.bfloat16), "tp", scatter_dimension=1, tiled=True
    )
    columns = features
    grad_conv_up = lax.psum_scatter(
        lax.dot_general(
            columns, d_up_a, (((0,), (0,)), ((), ())), preferred_element_type=jnp.float32
        ),
        "fs",
        scatter_dimension=0,
        tiled=True,
    )
    squares = jnp.sum(grad_conv_up * grad_conv_up, axis=0)
    placed = jnp.zeros((TAPS + 1, width * lax.axis_size("tp")), jnp.float32)
    placed = lax.dynamic_update_slice_in_dim(placed, column_part, col_start, 1)
    full_columns = lax.psum(placed, ("fs", "tp"))
    unit_norms = lax.psum(squares, "fs")
    return (grad_inputs, grad_conv_up, unit_norms, full_columns[:TAPS], full_columns[TAPS])


def ring_member(place, n):
    depth = n // 2
    place = lax.rem(place + 2 * n, n)
    side = place // depth
    along = lax.rem(place, depth)
    return (side * (depth - 1) + (1 - 2 * side) * along) * 2 + side


def ring_place(index, n):
    side = lax.rem(index, 2)
    along = index // 2
    return side * (n - 1 - 2 * along) + along


def greet(peers):
    barrier = pltpu.get_barrier_semaphore()
    for peer in peers:
        pl.semaphore_signal(barrier, inc=1, device_id=peer, device_id_type=MESH)
    pl.semaphore_wait(barrier, len(peers))


def gather_kernel(n, t, *refs):
    tokens, grown, projected = refs[3:5], refs[5:10], refs[10:13]
    w_out = refs[13:15] + grown[:4]
    t_out = (grown[4], refs[15])
    totals = refs[16:22]
    send_sem, recv_sem, t_send, t_recv = refs[22:]
    cut, rest = w_out[0].shape[2], w_out[1].shape[2]
    spans = (pl.ds(0, cut), pl.ds(cut, rest))
    weights = [w.at[:, span] for w in refs[:3] for span in spans]
    me, mine = lax.axis_index("fs"), lax.axis_index("tp")
    place = ring_place(me, n)
    ways = (
        {"fs": ring_member(place + 1, n)},
        {"fs": ring_member(place - 1, n)},
    )
    peers = [{"tp": lax.rem(mine + k, t)} for k in range(1, t)]
    blocks = tokens[0].shape[0]
    held = pl.ds(mine * blocks, blocks)
    greet(list(ways) + peers)

    def push(src, dst, send, recv, to):
        copy = pltpu.make_async_remote_copy(
            src_ref=src, dst_ref=dst, send_sem=send, recv_sem=recv,
            device_id=to, device_id_type=MESH,
        )
        copy.start()
        return copy

    def owner_of(i, step):
        return ring_member(place - step if i % 2 == 0 else place + step, n)

    def multiply(step, i):
        owner = owner_of(i, step)
        product = lax.dot_general(
            t_out[1 if i < 2 else 0][owner],
            w_out[i][owner],
            (((0,), (0,)), ((), ())),
            preferred_element_type=jnp.float32,
        )
        totals[i][...] = totals[i][...] + product if step else product

    first = min(3, n - 2)
    waiting = [(step, i) for step in range(n) for i in range(6)]
    ring = []
    for step in range(n - 1):
        copies = []
        for i in range(6):
            if step:
                ring[step - 1][i].wait_recv()
            owner = owner_of(i, step)
            copies.append(
                push(
                    w_out[i].at[owner] if step else weights[i],
                    w_out[i].at[owner],
                    send_sem.at[step, i],
                    recv_sem.at[step, i],
                    ways[i % 2],
                )
            )
            if step == first and i == 0:
                for copy in across:
                    copy.wait_recv()
            if step >= first:
                for _ in range(2):
                    if waiting[0] <= (step, i):
                        multiply(*waiting.pop(0))
        ring.append(copies)
        if step == 0:
            across = [
                push(
                    tokens[i],
                    t_out[i].at[held],
                    t_send.at[i, k - 1],
                    t_recv.at[i, k - 1],
                    peers[k - 1],
                )
                for i in range(2)
                for k in range(1, t)
            ]
            for i in range(6):
                w_out[i][me] = refs[i // 2][:, (i % 2) * cut : cut + (i % 2) * rest]
            for i in range(2):
                t_out[i][held] = tokens[i][...]
    for step, i in waiting:
        if step == n - 1:
            ring[-1][i].wait_recv()
        multiply(step, i)
    for i in range(6):
        projected[i // 2][:, (i % 2) * cut : cut + (i % 2) * rest] = totals[i][...].astype(
            jnp.bfloat16
        )
    for copies in ring + [across]:
        for copy in copies:
            copy.wait_send()


def gather_all(weights, tokens, cuts, n, t):
    shape, kind = jax.ShapeDtypeStruct, jnp.bfloat16
    shard, width = weights[0].shape
    rows = tokens[0].shape[1]
    tokens = [x.reshape(-1, shard, rows) for x in tokens]
    dma = pltpu.SemaphoreType.DMA
    return pl.pallas_call(
        functools.partial(gather_kernel, n, t),
        out_shape=[shape((n, shard, c), kind) for _ in range(2) for c in cuts]
        + [shape((n, shard, rows), kind)]
        + [shape((rows, width), kind)] * 3,
        in_specs=[VMEM] * 5,
        out_specs=[VMEM] * 8,
        scratch_shapes=[pltpu.VMEM((n, shard, c), kind) for c in cuts]
        + [pltpu.VMEM((n, shard, rows), kind)]
        + [pltpu.VMEM((rows, c), jnp.float32) for _ in range(3) for c in cuts]
        + [dma((n - 1, 6)), dma((n - 1, 6)), dma((2, t - 1)), dma((2, t - 1))],
        compiler_params=pltpu.CompilerParams(
            collective_id=0, has_side_effects=True, vmem_limit_bytes=56 * 1024 * 1024
        ),
        name="gather_all",
    )(*weights, *tokens)


def reduce_kernel(n, t, *refs):
    grads, partial, columns = refs[:2], refs[2], refs[3]
    g_out, i_out, norm_out, col_out = refs[4:8]
    sent, held = refs[8:10], refs[10:12]
    arrived, col_all, col_sum, norm_own, norm_all = refs[12:17]
    (send_sem, recv_sem, t_send, t_recv, c_send, c_recv, s_send, s_recv, n_send, n_recv) = refs[17:]
    parts = grads[0].shape[1]
    me, mine = lax.axis_index("fs"), lax.axis_index("tp")
    place = ring_place(me, n)
    ways = (
        {"fs": ring_member(place + 1, n)},
        {"fs": ring_member(place - 1, n)},
    )
    peers = [{"tp": lax.rem(mine + k, t)} for k in range(1, t)]
    column = [{"fs": lax.rem(me + k, n)} for k in range(1, n)]
    greet(column + peers)

    def push(src, dst, send, recv, to):
        copy = pltpu.make_async_remote_copy(
            src_ref=src, dst_ref=dst, send_sem=send, recv_sem=recv,
            device_id=to, device_id_type=MESH,
        )
        copy.start()
        return copy

    col_pushes = [
        push(columns, col_all.at[me], c_send.at[k], c_recv.at[k], column[k])
        for k in range(n - 1)
    ]
    across = [
        push(
            partial.at[lax.rem(mine + k, t)],
            arrived.at[k - 1],
            t_send.at[k - 1],
            t_recv.at[k - 1],
            peers[k - 1],
        )
        for k in range(1, t)
    ]
    ring = []
    for step in range(n - 1):
        copies = []
        for c in range(parts):
            for way in range(2):
                ahead = place - 1 - step if way == 0 else place + 1 + step
                value = grads[way][ring_member(ahead, n), c]
                slot = c * 2 + way
                if step:
                    ring[step - 1][slot].wait_recv()
                    value = value + held[way][step - 1, c].astype(jnp.float32)
                sent[way][step, c] = value.astype(jnp.bfloat16)
                copies.append(
                    push(
                        sent[way].at[step, c],
                        held[way].at[step, c],
                        send_sem.at[step, slot],
                        recv_sem.at[step, slot],
                        ways[way],
                    )
                )
        ring.append(copies)
        if step == 1:
            for copy in col_pushes:
                copy.wait_recv()
            total = jnp.zeros(columns.shape, jnp.float32)
            for k in range(n):
                total = total + jnp.where(me == k, columns[...], col_all[k])
            col_sum[...] = total
            col_out[mine] = total
            sum_pushes = [
                push(col_sum, col_out.at[mine], s_send.at[k], s_recv.at[k], peers[k])
                for k in range(t - 1)
            ]
    for copy in across:
        copy.wait_recv()
    rows = partial.shape[1]
    piece = 16 if rows % 16 == 0 else 8

    @pl.loop(0, rows // piece)
    def _(r):
        at = pl.ds(pl.multiple_of(r * piece, piece), piece)
        total = partial[mine, at, :].astype(jnp.float32)
        for k in range(t - 1):
            total = total + arrived[k, at, :].astype(jnp.float32)
        i_out[at, :] = total.astype(jnp.bfloat16)

    height = grads[0].shape[2]
    start = 0
    for way in range(2):
        lanes = grads[way].shape[3]
        squares = jnp.zeros((1, lanes), jnp.float32)
        for c in range(parts):
            slot = c * 2 + way
            ring[-1][slot].wait_recv()
            value = grads[way][me, c] + held[way][n - 2, c].astype(jnp.float32)
            g_out[c * height : (c + 1) * height, start : start + lanes] = value
            squares = squares + jnp.sum(value * value, axis=0, keepdims=True)
        norm_own[:, start : start + lanes] = squares
        start += lanes
    norm_pushes = [
        push(norm_own, norm_all.at[me], n_send.at[k], n_recv.at[k], column[k])
        for k in range(n - 1)
    ]
    for copy in norm_pushes:
        copy.wait_recv()
    total = jnp.zeros(norm_own.shape, jnp.float32)
    for k in range(n):
        total = total + jnp.where(me == k, norm_own[...], norm_all[k])
    norm_out[...] = total
    for copy in sum_pushes:
        copy.wait_recv()
    for copies in ring + [across, col_pushes, sum_pushes, norm_pushes]:
        for copy in copies:
            copy.wait_send()


def reduce_all(grads, partial, columns, n, t):
    shape = jax.ShapeDtypeStruct
    parts, rows = grads[0].shape[1:3]
    width = sum(g.shape[3] for g in grads)
    dma = pltpu.SemaphoreType.DMA
    blocks = [pltpu.VMEM((n - 1,) + g.shape[1:], jnp.bfloat16) for g in grads]
    return pl.pallas_call(
        functools.partial(reduce_kernel, n, t),
        out_shape=[
            shape((parts * rows, width), jnp.float32),
            shape(partial.shape[1:], jnp.bfloat16),
            shape((1, width), jnp.float32),
            shape((t,) + columns.shape, jnp.float32),
        ],
        in_specs=[VMEM] * 4,
        out_specs=[VMEM] * 4,
        scratch_shapes=[
            *blocks,
            *blocks,
            pltpu.VMEM((t - 1,) + partial.shape[1:], jnp.bfloat16),
            pltpu.VMEM((n,) + columns.shape, jnp.float32),
            pltpu.VMEM(columns.shape, jnp.float32),
            pltpu.VMEM((1, width), jnp.float32),
            pltpu.VMEM((n, 1, width), jnp.float32),
            dma((n - 1, 2 * parts)),
            dma((n - 1, 2 * parts)),
            dma((t - 1,)),
            dma((t - 1,)),
            dma((n - 1,)),
            dma((n - 1,)),
            dma((t - 1,)),
            dma((t - 1,)),
            dma((n - 1,)),
            dma((n - 1,)),
        ],
        compiler_params=pltpu.CompilerParams(
            collective_id=1, has_side_effects=True, vmem_limit_bytes=56 * 1024 * 1024
        ),
        name="reduce_all",
    )(*grads, partial, columns)


def halo_kernel(n, block, out, send_sem, recv_sem):
    me = lax.axis_index("fs")
    before, after = {"fs": lax.rem(me + n - 1, n)}, {"fs": lax.rem(me + 1, n)}
    greet([before, after])
    copy = pltpu.make_async_remote_copy(
        src_ref=block, dst_ref=out, send_sem=send_sem, recv_sem=recv_sem,
        device_id=before, device_id_type=MESH,
    )
    copy.start()
    copy.wait()


def from_next(block, n):
    got = pl.pallas_call(
        functools.partial(halo_kernel, n),
        out_shape=jax.ShapeDtypeStruct(block.shape, block.dtype),
        in_specs=[VMEM],
        out_specs=VMEM,
        scratch_shapes=[pltpu.SemaphoreType.DMA, pltpu.SemaphoreType.DMA],
        compiler_params=pltpu.CompilerParams(
            collective_id=2, has_side_effects=True, vmem_limit_bytes=1024 * 1024
        ),
        name="from_next",
    )(block)
    return jnp.where(lax.axis_index("fs") == n - 1, 0.0, got)


def with_kernels(inputs, w_conv_up, w_gate_up, w_down, taps, conv_bias, cotangent):
    n, t = lax.axis_size("fs"), lax.axis_size("tp")
    span = TAPS - 1
    rows = inputs.shape[0]
    shard, width = w_conv_up.shape
    half = -(-width // (2 * LANES)) * LANES
    col_start = lax.axis_index("tp") * width
    cuts = (half, width - half)
    starts = ((0, half), (half, width))
    taps_own = lax.dynamic_slice_in_dim(taps, col_start, width, 1)
    bias_own = lax.dynamic_slice_in_dim(conv_bias, col_start, width, 0)
    got = gather_all([w_down.T, w_conv_up, w_gate_up], [inputs.T, cotangent.T], cuts, n, t)
    conv, gate = [[g.reshape(n * shard, -1) for g in got[i : i + 2]] for i in (0, 2)]
    features = got[4].reshape(-1, rows)
    d_hidden, up_a, up_b = got[5:]
    earlier = shifted(up_a[rows - span :], "fs", 1)
    extended = jnp.concatenate([earlier, up_a], 0).astype(jnp.float32)
    conv_out = bias_own[None, :] + sum(
        (taps_own[i][None, :] * extended[i : i + rows] for i in range(TAPS))
    )
    gelu_value, gelu_slope = gelu_parts(conv_out)
    hidden_grad = d_hidden.astype(jnp.float32)
    d_conv = hidden_grad * up_b.astype(jnp.float32) * gelu_slope
    d_up_b = (hidden_grad * gelu_value).astype(jnp.bfloat16)
    later = from_next(d_conv[:8], n)[:span]
    d_extended = jnp.concatenate([d_conv, later], 0)
    d_up_a = sum(
        (taps_own[i][None, :] * d_extended[span - i : span - i + rows] for i in range(TAPS))
    ).astype(jnp.bfloat16)
    tap_terms = [jnp.sum(d_conv * extended[i : i + rows], axis=0) for i in range(TAPS)]
    column_part = jnp.stack(tap_terms + [jnp.sum(d_conv, axis=0)], 0)
    partial_sum = 0.0
    for weight, grad in ((conv, d_up_a), (gate, d_up_b)):
        for h in range(2):
            partial_sum = partial_sum + lax.dot_general(
                weight[h],
                grad[:, slice(*starts[h])],
                (((1,), (1,)), ((), ())),
                preferred_element_type=jnp.float32,
            )
    partial = partial_sum.astype(jnp.bfloat16).reshape(t, -1, rows)
    parts = next(p for p in (3, 4, 2, 1) if shard % (8 * p) == 0)
    grads = [
        jnp.dot(
            features, d_up_a[:, slice(*starts[h])], preferred_element_type=jnp.float32
        ).reshape(n, parts, shard // parts, cuts[h])
        for h in range(2)
    ]
    grad_conv_up, grad_inputs, norms, columns = reduce_all(grads, partial, column_part, n, t)
    full = columns.transpose(1, 0, 2).reshape(TAPS + 1, t * width)
    return (grad_inputs.T, grad_conv_up, norms[0], full[:TAPS], full[TAPS])


def per_device(inputs, w_conv_up, *rest):
    n, t = lax.axis_size("fs"), lax.axis_size("tp")
    aligned = w_conv_up.shape[0] % 8 == 0 and inputs.shape[1] % w_conv_up.shape[0] == 0
    small = n % 2 == 0 and 4 <= n <= 16 and 2 <= t <= 8
    chosen = with_kernels if aligned and small else with_collectives
    return chosen(inputs, w_conv_up, *rest)


def solution(mesh):
    return jax.shard_map(
        per_device,
        mesh=mesh,
        in_specs=(
            P("fs", "tp"),
            P("fs", "tp"),
            P("fs", "tp"),
            P("tp", "fs"),
            P(),
            P(),
            P("fs", "tp"),
        ),
        out_specs=(P("fs", "tp"), P("fs", "tp"), P("tp"), P(), P()),
        check_vma=False,
    )
```

profile of v0, /device:TPU:0, one launch (start us, length us, event | category | flops | bytes accessed | tf_op | source)
XLA Modules:
  0.0 187.3 jit_solution(11072292679934279530)
XLA Ops:
  0.6 98.2 %gather_all.1 = (bf16[8,264,384]{2,1,0:T(8,128)(2,1)}, bf16[8,264,320]{2,1,0:T(8,128)(2,1)}, bf16[8,264,384]{2,1,0:T(8,128)(2,1)}, bf16[8,264,320]{2,1,0:T(8,128...) custom-call(bf16[264,704]{1,0:T(8,128)(2,1)} %bitcast.40, ...), custom_call_target="tpu_custom_call" | custom-call | tf_op jit(solution)/shard_map/gather_all/pallas_call | solution.py:218
  98.8 0.0 copy-start.2
  98.8 0.0 copy-start.7
  98.8 0.8 slice.64
  99.7 3.5 %collective-permute-start = (bf16[2,704]{1,0:T(2,128)(2,1)S(1)}, bf16[2,704]{1,0:T(2,128)(2,1)S(1)}, u32[]{:S(2)}, u32[]{:S(2)}) collective-permute-start(bf16[2,704]{1,0:T(2,128)(2,1)S(1)} %slice.64), channel_id=1, source_target_pairs={{0,4},{4,8},{8,12},{12,16},{16,20},{20,24},{24,28},{1,5},{5,9},{9,... | collective-permute-start | bytes 8456 | tf_op jit(solution)/shard_map/ppermute | solution.py:21
  103.1 0.8 dynamic_slice.7
  103.9 0.9 dynamic-slice_reduce_fusion.2
  104.8 0.0 collective-permute-done
  104.8 1.3 maximum_convert_fusion
  106.1 0.0 copy-done.2
  106.2 1.8 multiply_reduce_fusion.2
  108.0 5.4 %from_next.1 = f32[8,704]{1,0:T(8,128)S(1)} custom-call(f32[8,704]{1,0:T(8,128)S(1)} %slice.84.block), custom_call_target="tpu_custom_call" | custom-call | tf_op jit(solution)/shard_map/from_next/pallas_call | solution.py:407
  113.4 1.1 fusion.5
  114.6 0.5 copy-done
  115.0 3.0 %fusion.17.refs_1_ = f32[8,3,88,320]{3,2,1,0:T(8,128)} fusion(bf16[8,3,88,512]{3,2,1,0:T(8,128)(2,1)S(1)} %bitcast.30, bf16[512,704]{1,0:T(8,128)(2,1)S(1)} %get-tuple-element.38), kind=kOutput, calls=%fused_computation.32 | convolution fusion | flops 692060160 | bytes 5259264 | tf_op jit(solution)/shard_map/dot_general | solution.py:464
  118.1 3.0 %fusion.15.refs_0_ = f32[8,3,88,384]{3,2,1,0:T(8,128)} fusion(bf16[8,3,88,512]{3,2,1,0:T(8,128)(2,1)S(1)} %bitcast.31, bf16[512,704]{1,0:T(8,128)(2,1)S(1)} %get-tuple-element.38), kind=kOutput, calls=%fused_computation.30 | convolution fusion | flops 830472192 | bytes 5799936 | tf_op jit(solution)/shard_map/dot_general | solution.py:464
  121.1 1.3 fusion.21
  122.4 0.1 copy-done.5
  122.5 1.4 convolution_add_fusion.2
  123.9 0.0 copy-done.4
  123.9 1.3 convolution_add_fusion.1
  125.2 0.1 copy-done.3
  125.3 2.7 %fusion = bf16[2112,512]{1,0:T(8,128)(2,1)} fusion(f32[2112,512]{1,0:T(8,128)S(1)} %convolution_add_fusion.1, bf16[2112,320]{1,0:T(8,128)(2,1)S(1)} %bitcast.34, bf16[512,704]{1,0:T(8,128)(2,1)S(1)} %get-tuple-element.39), kind=kOutput, calls=%fused_computation.3 | convolution fusion | flops 694222848 | bytes 8503296 | tf_op jit(solution)/shard_map/dot_general | solution.py:455
  128.0 0.6 pad_maximum_fusion.1.refs_3_
  128.6 51.5 %reduce_all.1 = (f32[264,704]{1,0:T(8,128)}, bf16[528,512]{1,0:T(8,128)(2,1)}, f32[1,704]{1,0:T(1,128)}, f32[4,4,704]{2,1,0:T(4,128)}) custom-call(f32[8,3,88,384]{3,2,1,0:T(8,128)} %fusion.15.refs_0_, f32[8,3,88,320]{3,2,1,0:T(8,128)} %fusion.17.refs_1_, bf16[4,528,512]{2,1,0:T(8,128)(2,1)} %bitcast.32, f32[4,704]{1,0:T(4,128)} %pad_maximum_fusion.1.refs_3_), custom_call_target="tpu_custom_call" | custom-call | tf_op jit(solution)/shard_map/reduce_all/pallas_call | solution.py:358
  180.1 0.9 slice_reduce_fusion
  181.0 0.7 squeeze.7
  181.7 0.8 copy.14
  182.5 0.7 slice.79
  183.3 1.3 reduce.3
  184.5 1.9 %copy.20 = bf16[512,528]{0,1:T(8,128)(2,1)} copy(bf16[512,528]{0,1:T(8,128)(2,1)} %bitcast.39) | data formatting | bytes 1081344
  186.4 0.9 copy.21
  (15 shorter events, 0.0 us)
Async XLA Ops:
  98.8 7.3 %copy-start.2 = (bf16[512,704]{1,0:T(8,128)(2,1)S(1)}, bf16[512,704]{1,0:T(8,128)(2,1)}, u32[]{:S(2)}) copy-start(bf16[512,704]{1,0:T(8,128)(2,1)} %get-tuple-element.18) | copy-start | bytes 2162692
  98.8 7.3 %copy-start.7 = (bf16[512,704]{1,0:T(8,128)(2,1)S(1)}, bf16[512,704]{1,0:T(8,128)(2,1)}, u32[]{:S(2)}) copy-start(bf16[512,704]{1,0:T(8,128)(2,1)} %get-tuple-element.19) | copy-start | bytes 2162692
  99.7 5.2 %collective-permute-start = (bf16[2,704]{1,0:T(2,128)(2,1)S(1)}, bf16[2,704]{1,0:T(2,128)(2,1)S(1)}, u32[]{:S(2)}, u32[]{:S(2)}) collective-permute-start(bf16[2,704]{1,0:T(2,128)(2,1)S(1)} %slice.64), channel_id=1, source_target_pairs={{0,4},{4,8},{8,12},{12,16},{16,20},{20,24},{24,28},{1,5},{5,9},{9,... | collective-permute-start | bytes 8456 | tf_op jit(solution)/shard_map/ppermute | solution.py:21
  113.4 1.6 copy-start
  118.0 3.0 %copy-start.1 = (bf16[8,264,384]{2,1,0:T(8,128)(2,1)S(1)}, bf16[8,264,384]{2,1,0:T(8,128)(2,1)}, u32[]{:S(2)}) copy-start(bf16[8,264,384]{2,1,0:T(8,128)(2,1)} %get-tuple-element.21) | copy-start | bytes 4866052
  121.1 1.4 copy-start.5
  122.5 1.4 copy-start.4
  123.9 1.4 copy-start.3
  180.1 6.3 %copy-start.6 = (f32[264,704]{1,0:T(8,128)S(1)}, f32[264,704]{1,0:T(8,128)}, u32[]{:S(2)}) copy-start(f32[264,704]{1,0:T(8,128)} %get-tuple-element.46) | copy-start | bytes 2230276
where the time goes:
time: 188 us; the launch traced here: 187 us
  Pallas kernels  155 us (82%)
  matrix products  12.7 us (7%)
  local copies, waits for them, and re-layouts  9.17 us (5%)
  other arithmetic  6.1 us (3%)
  starting transfers between devices  3.46 us (2%)
    pallas_call x1, Pallas kernels, gather_all(): pl.pallas_call(functools.partial(gather_kernel, n, t), out_shape=[shape((...  98.2 us
    pallas_call x1, Pallas kernels, reduce_all(): pl.pallas_call(functools.partial(reduce_kernel, n, t), out_shape=[shape((...  51.5 us
    dot_general x4, matrix products, with_kernels(): lax.dot_general(weight[h], grad[:, slice(*starts[h])], (((1,), (1,)), (()...  6.7 us
    dot_general x2, matrix products, with_kernels(): jnp.dot(features, d_up_a[:, slice(*starts[h])], preferred_element_type=jn...  5.98 us
    pallas_call x1, Pallas kernels, from_next(): pl.pallas_call(functools.partial(halo_kernel, n), out_shape=jax.ShapeDtyp...  5.44 us
  transfers between devices with their start and end apart: 1, of which 0 were waited for; matrix products, arithmetic and copies ran while one was open for 1% of the time, Pallas kernels for 0%

commit v1 on v0

v1 whole, which is shorter than its diff:
```python
import functools
import math

import jax
import jax.numpy as jnp
from jax import lax
from jax.experimental import pallas as pl
from jax.experimental.pallas import tpu as pltpu
from jax.sharding import PartitionSpec as P

TAPS = 3
LANES = 128
MESH = pl.DeviceIdType.MESH
VMEM = pl.BlockSpec(memory_space=pltpu.VMEM)
ANY = pl.BlockSpec(memory_space=pl.ANY)


def shifted(block, axis, distance):
    devices = range(lax.axis_size(axis))
    route = [(i - distance, i) for i in devices if i - distance in devices]
    return lax.ppermute(block, axis, route)


def gelu_parts(value):
    normal_cdf = 0.5 * (1.0 + jax.scipy.special.erf(value / math.sqrt(2.0)))
    density = jnp.exp(-0.5 * value * value) / math.sqrt(2.0 * math.pi)
    return (value * normal_cdf, normal_cdf + value * density)


def with_collectives(inputs, w_conv_up, w_gate_up, w_down, taps, conv_bias, cotangent):
    span = TAPS - 1
    rows = inputs.shape[0]
    width = w_conv_up.shape[1]
    col_start = lax.axis_index("tp") * width
    taps_own = lax.dynamic_slice_in_dim(taps, col_start, width, 1)
    bias_own = lax.dynamic_slice_in_dim(conv_bias, col_start, width, 0)
    features, cot_full = (
        lax.all_gather(inputs, "tp", axis=1, tiled=True),
        lax.all_gather(cotangent, "tp", axis=1, tiled=True),
    )
    conv_weight, gate_weight = (
        lax.all_gather(w_conv_up, "fs", axis=0, tiled=True),
        lax.all_gather(w_gate_up, "fs", axis=0, tiled=True),
    )
    columns = cot_full
    d_hidden = lax.dot_general(
        columns,
        lax.all_gather(w_down, "fs", axis=1, tiled=True),
        (((1,), (1,)), ((), ())),
        preferred_element_type=jnp.float32,
    ).astype(jnp.bfloat16)
    up_a = jnp.dot(features, conv_weight, preferred_element_type=jnp.float32).astype(jnp.bfloat16)
    up_b = jnp.dot(features, gate_weight, preferred_element_type=jnp.float32).astype(jnp.bfloat16)
    earlier = shifted(up_a[rows - span :], "fs", 1)
    extended = jnp.concatenate([earlier, up_a], 0).astype(jnp.float32)
    conv_out = bias_own[None, :] + sum(
        (taps_own[i][None, :] * extended[i : i + rows] for i in range(TAPS))
    )
    gelu_value, gelu_slope = gelu_parts(conv_out)
    hidden_grad = d_hidden.astype(jnp.float32)
    d_conv = hidden_grad * up_b.astype(jnp.float32) * gelu_slope
    d_up_b = (hidden_grad * gelu_value).astype(jnp.bfloat16)
    later = shifted(d_conv[:span], "fs", -1)
    d_extended = jnp.concatenate([d_conv, later], 0)
    d_up_a = sum(
        (taps_own[i][None, :] * d_extended[span - i : span - i + rows] for i in range(TAPS))
    ).astype(jnp.bfloat16)
    tap_terms = [jnp.sum(d_conv * extended[i : i + rows], axis=0) for i in range(TAPS)]
    column_part = jnp.stack(tap_terms + [jnp.sum(d_conv, axis=0)], 0)
    contract = (((1,), (1,)), ((), ()))
    partial_sum = lax.dot_general(d_up_a, conv_weight, contract, preferred_element_type=jnp.float32)
    partial_sum = partial_sum + lax.dot_general(
        d_up_b, gate_weight, contract, preferred_element_type=jnp.float32
    )
    grad_inputs = lax.psum_scatter(
        partial_sum.astype(jnp.bfloat16), "tp", scatter_dimension=1, tiled=True
    )
    columns = features
    grad_conv_up = lax.psum_scatter(
        lax.dot_general(
            columns, d_up_a, (((0,), (0,)), ((), ())), preferred_element_type=jnp.float32
        ),
        "fs",
        scatter_dimension=0,
        tiled=True,
    )
    squares = jnp.sum(grad_conv_up * grad_conv_up, axis=0)
    placed = jnp.zeros((TAPS + 1, width * lax.axis_size("tp")), jnp.float32)
    placed = lax.dynamic_update_slice_in_dim(placed, column_part, col_start, 1)
    full_columns = lax.psum(placed, ("fs", "tp"))
    unit_norms = lax.psum(squares, "fs")
    return (grad_inputs, grad_conv_up, unit_norms, full_columns[:TAPS], full_columns[TAPS])


def greet(peers):
    barrier = pltpu.get_barrier_semaphore()
    for peer in peers:
        pl.semaphore_signal(barrier, inc=1, device_id=peer, device_id_type=MESH)
    pl.semaphore_wait(barrier, len(peers))


def dot(a, b, da, db):
    return lax.dot_general(
        a, b, (((da,), (db,)), ((), ())), preferred_element_type=jnp.float32
    )


def rounded(value):
    return value.astype(jnp.bfloat16).astype(jnp.float32)


def buffers(n, t, shard, rows, ca):
    b16, f32 = jnp.bfloat16, jnp.float32
    return dict(
        stage=pltpu.VMEM((3, shard, ca), b16),
        wbuf=pltpu.VMEM((3, n, shard, ca), b16),
        abuf=pltpu.VMEM((2, 2, n, shard, rows), b16),
        tot=pltpu.VMEM((3, 2, rows + 8, ca), f32),
        halo_up=pltpu.VMEM((2, 8, ca), f32),
        halo_dc=pltpu.VMEM((2, 8, ca), f32),
        tb=pltpu.VMEM((8, ca), f32),
        dcv=pltpu.VMEM((2, rows + 8, ca), f32),
        dup=pltpu.VMEM((2, 2, rows, ca), b16),
        col_own=pltpu.VMEM((8, ca), f32),
        col_got=pltpu.VMEM((3, 8, ca), f32),
        col_sum=pltpu.VMEM((8, ca), f32),
        col_all=pltpu.VMEM((t, 2, 8, ca), f32),
        ysend=pltpu.VMEM((4, shard, ca), b16),
        yrecv=pltpu.VMEM((4, shard, ca), b16),
        gown=pltpu.VMEM((4, shard, ca), f32),
        zsend=pltpu.VMEM((3, shard, ca), b16),
        zrecv=pltpu.VMEM((4, shard, ca), b16),
        csend=pltpu.VMEM((8, shard, rows), b16),
        crecv=pltpu.VMEM((8, shard, rows), b16),
        pown=pltpu.VMEM((8, shard, rows), f32),
        xsend=pltpu.VMEM((4, shard, rows), b16),
        xrecv=pltpu.VMEM((4, shard, rows), b16),
        psend=pltpu.VMEM((2, shard, rows), b16),
        precv=pltpu.VMEM((2, shard, rows), b16),
        norm_own=pltpu.VMEM((8, ca), f32),
        norm_all=pltpu.VMEM((n, 8, ca), f32),
    )


def semaphores(n, t):
    shapes = dict(
        wz=(3, 3), wy=(3, 4), az=(4,), ax=(2, 4), ac=(4, 4), hu=(2,), hd=(2,),
        c1=(3,), c2=(2 * t - 1,), gy=(4,), gz=(4,), pc=(8,), px=(4,), pz=(2,), nm=(n - 1,),
    )
    dma = pltpu.SemaphoreType.DMA
    return {name + end: dma(s) for name, s in shapes.items() for end in ("_s", "_r")}


def layer_kernel(n, t, names, *refs):
    w, acts, taps, bias = refs[:3], refs[3:5], refs[5], refs[6]
    i_out, g_out, norm_out, taps_out, bias_out = refs[7:12]
    m = dict(zip(names, refs[12:]))
    stage, wbuf, abuf, tot = m["stage"], m["wbuf"], m["abuf"], m["tot"]
    dcv, dup, tb = m["dcv"], m["dup"], m["tb"]
    shard, width = w[0].shape
    ca = stage.shape[2]
    cb = width - ca
    rows = acts[0].shape[2]
    me, mine = lax.axis_index("fs"), lax.axis_index("tp")
    z, y = me // 2, lax.rem(me, 2)
    x, c = mine // 2, lax.rem(mine, 2)
    l = lax.rem(z, 2)
    upper = z // 2
    zp = z + 1 - 2 * l
    zo = 3 - z
    far = 3 - zp
    inner_i = lax.rem((z + 1) // 2, 2)
    inner = inner_i == 1
    outer = inner_i == 0
    across = {"fs": z * 2 + 1 - y}
    pair = {"fs": zp * 2 + y}
    x_dev = {"tp": (1 - x) * 2 + c}
    twin = {"tp": x * 2 + 1 - c}
    x_tp = (1 - x) * 2 + c
    line = [zp, far, zo]
    started = []

    def copy(name, at, src, dst, to, slot=None):
        slot = at if slot is None else slot
        return pltpu.make_async_remote_copy(
            src_ref=src, dst_ref=dst,
            send_sem=m[name + "_s"].at[at], recv_sem=m[name + "_r"].at[slot],
            device_id=to, device_id_type=MESH,
        )

    def push(*args, **kw):
        made = copy(*args, **kw)
        made.start()
        started.append(made)
        return made

    def put(i, ref, first):
        if first:
            ref[...] = w[i][:, :ca]
        else:
            ref[:, cb // LANES * LANES :] = jnp.zeros(
                (shard, ca - cb // LANES * LANES), jnp.bfloat16
            )
            ref[:, :cb] = w[i][:, ca:]

    for i in range(3):
        for flag, first in ((inner, True), (outer, False)):
            @pl.when(flag)
            def _(i=i, first=first):
                put(i, wbuf.at[i, me], first)
                put(i, stage.at[i], not first)
    for a in range(2):
        for half in range(2):
            abuf[a, l, 2 * mine + half] = acts[a][half]
    tb[...] = jnp.zeros(tb.shape, jnp.float32)
    for p in range(t):
        for flag, start, size in ((inner, 0, ca), (outer, ca, cb)):
            @pl.when(jnp.logical_and(mine == p, flag))
            def _(p=p, start=start, size=size):
                at = p * width + start
                tb[0:3, 0:size] = taps[:, at : at + size]
                tb[3:4, 0:size] = bias[:, at : at + size]

    others = [{"fs": lax.rem(me + k, n)} for k in range(1, n)]
    others += [{"tp": lax.rem(mine + k, t)} for k in range(1, t)]
    others += [{"fs": zp * 2 + y, "tp": lax.rem(mine + k, t)} for k in range(1, t)]
    greet(others)

    quarter = [(1, 0), (1, 1), (0, 0), (0, 1)]
    own_act = [abuf.at[a, l, 2 * mine + half] for a, half in quarter]
    pair_act = [abuf.at[a, 1 - l, 2 * mine + half] for a, half in quarter]
    x_act = [abuf.at[a, l, 2 * x_tp + half] for a, half in quarter]
    xp_act = [abuf.at[a, 1 - l, 2 * x_tp + half] for a, half in quarter]
    az, ax, ac, wz, wy = {}, {}, {}, {}, {}

    def send_act(q):
        a, half = quarter[q]
        az[q] = push("az", (q,), acts[a].at[half], own_act[q], pair)
        ax[0, q] = push("ax", (0, q), acts[a].at[half], own_act[q], x_dev)
        ac[0, q] = push("ac", (0, q), acts[a].at[half], own_act[q], twin)

    def send_w(i):
        own = wbuf.at[i, me]
        for j in range(3):
            wz[i, j] = push(
                "wz", (i, j), own if j == 2 else stage.at[i], own, {"fs": line[j] * 2 + y}
            )
        wy[i, 3] = push("wy", (i, 3), own, own, across)

    def pass_w(i, j):
        wz[i, j].wait_recv()
        slot = wbuf.at[i, line[j] * 2 + y]
        wy[i, j] = push("wy", (i, j), slot, slot, across)

    def pass_pair(q):
        az[q].wait_recv()
        ax[1, q] = push("ax", (1, q), pair_act[q], pair_act[q], x_dev)
        ac[1, q] = push("ac", (1, q), pair_act[q], pair_act[q], twin)

    def pass_x(way, q):
        ax[way, q].wait_recv()
        ref = (x_act, xp_act)[way][q]
        ac[2 + way, q] = push("ac", (2 + way, q), ref, ref, twin)

    def multiply(i, zz, fresh):
        a = 1 if i == 0 else 0

        @pl.loop(0, 2)
        def _(b):
            product = dot(abuf[a, b, 2 * zz], wbuf[i, 2 * zz], 0, 0)
            product = product + dot(abuf[a, b, 2 * zz + 1], wbuf[i, 2 * zz + 1], 0, 0)
            if fresh:
                tot[i, b, 8:, :] = product
            else:
                tot[i, b, 8:, :] = tot[i, b, 8:, :] + product

    send_act(0)
    send_act(1)
    send_w(0)
    send_act(2)
    send_w(1)
    send_act(3)
    send_w(2)
    pass_pair(0)
    pass_x(0, 0)
    pass_x(0, 1)
    pass_pair(1)
    for j in range(3):
        pass_w(0, j)
    pass_x(0, 2)
    pass_x(0, 3)
    pass_x(1, 0)
    pass_pair(2)
    pass_x(1, 1)
    for j in range(3):
        pass_w(1, j)
    pass_pair(3)
    pass_x(1, 2)
    for s in range(4):
        for q in range(2):
            ac[s, q].wait_recv()
    for k, j in enumerate((3, 0, 1, 2)):
        wy[0, j].wait_recv()
        multiply(0, z if j == 3 else line[j], k == 0)
    pass_x(1, 3)
    for s in range(4):
        for q in range(2, 4):
            ac[s, q].wait_recv()
    for k, j in enumerate((3, 0, 1, 2)):
        wy[1, j].wait_recv()
        multiply(1, z if j == 3 else line[j], k == 0)
    for b in range(2):
        edge, where = tot.at[1, b, pl.ds(rows, 8)], m["halo_up"]
        if b == 0:
            hu0 = push("hu", (0,), edge, where.at[y], across, slot=(y,))
        else:
            hu_near = copy("hu", (1,), edge, where.at[1], across)
            hu_far = copy("hu", (1,), edge, where.at[0], {"fs": zo * 2}, slot=(0,))
            pl.when(y == 0)(hu_near.start)
            pl.when(jnp.logical_and(y == 1, upper == 0))(hu_far.start)
    for j in range(3):
        pass_w(2, j)

    span = 32
    steps = rows // span

    def row(k):
        return tb[k : k + 1, :]

    def gelu_rows(b, r):
        at = pl.multiple_of(r * span, span)
        around = rounded(tot[1, b, pl.ds(at, span + 8), :])
        value = row(3) + row(0) * around[6 : 6 + span]
        value = value + row(1) * around[7 : 7 + span] + row(2) * around[8 : 8 + span]
        cdf = 0.5 * (1.0 + lax.erf(value * (1.0 / math.sqrt(2.0))))
        density = jnp.exp(-0.5 * value * value) * (1.0 / math.sqrt(2.0 * math.pi))
        hidden = rounded(tot[0, b, pl.ds(at + 8, span), :])
        dup[1, b, pl.ds(at, span), :] = (hidden * (value * cdf)).astype(jnp.bfloat16)
        dcv[b, pl.ds(at, span), :] = hidden * (cdf + value * density)

    @pl.loop(0, 2 * (steps - 1))
    def _(k):
        gelu_rows(lax.rem(k, 2), 1 + k // 2)

    has_before = jnp.logical_or(y == 1, upper == 1)
    has_after = jnp.logical_or(y == 1 - 0, y == 0)
    del has_after
    wait_up = [copy("hu", (b,), m["halo_up"].at[b], m["halo_up"].at[b], across) for b in range(2)]
    wait_up[1].wait_recv()
    pl.when(has_before)(wait_up[0].wait_recv)
    tot[1, 1, 0:8, :] = m["halo_up"][1]

    @pl.when(has_before)
    def _():
        tot[1, 0, 0:8, :] = m["halo_up"][0]

    @pl.when(jnp.logical_not(has_before))
    def _():
        tot[1, 0, 0:8, :] = jnp.zeros((8, ca), jnp.float32)

    @pl.loop(0, 2)
    def _(b):
        gelu_rows(b, 0)

    for k, j in enumerate((3, 0, 1, 2)):
        wy[2, j].wait_recv()
        multiply(2, z if j == 3 else line[j], k == 0)

    def grad_rows(b, r, sums):
        at = pl.multiple_of(r * span, span)
        grad = dcv[b, pl.ds(at, span), :] * rounded(tot[2, b, pl.ds(at + 8, span), :])
        dcv[b, pl.ds(at, span), :] = grad
        around = rounded(tot[1, b, pl.ds(at, span + 8), :])

        def folded(value):
            total = value[0:8]
            for k in range(8, span, 8):
                total = total + value[k : k + 8]
            return total

        terms = [folded(grad * around[6 + i : 6 + i + span]) for i in range(3)] + [folded(grad)]
        return tuple(s + v for s, v in zip(sums, terms))

    sums = tuple(jnp.zeros((8, ca), jnp.float32) for _ in range(4))
    sums = lax.fori_loop(0, 2, lambda b, s: grad_rows(b, 0, s), sums)
    edge = dcv.at[0, pl.ds(0, 8)]
    hd_near = copy("hd", (0,), edge, m["halo_dc"].at[0], across)
    hd_far = copy("hd", (0,), edge, m["halo_dc"].at[1], {"fs": zo * 2 + 1}, slot=(1,))
    pl.when(y == 1)(hd_near.start)
    pl.when(jnp.logical_and(y == 0, upper == 1))(hd_far.start)
    push("hd", (1,), dcv.at[1, pl.ds(0, 8)], m["halo_dc"].at[y], across, slot=(y,))
    sums = lax.fori_loop(
        0, 2 * (steps - 1), lambda k, s: grad_rows(lax.rem(k, 2), 1 + k // 2, s), sums
    )
    m["col_own"][4:8, :] = jnp.zeros((4, ca), jnp.float32)
    for k in range(4):
        m["col_own"][k : k + 1, :] = jnp.sum(sums[k], axis=0, keepdims=True)
    group = [across, {"fs": zo * 2 + y}, {"fs": zo * 2 + 1 - y}]
    c1 = [push("c1", (k,), m["col_own"], m["col_got"].at[k], group[k]) for k in range(3)]

    def shift_rows(b, r):
        at = pl.multiple_of(r * span, span)
        ahead = dcv[b, pl.ds(at, span + 8), :]
        total = row(0) * ahead[2 : 2 + span] + row(1) * ahead[1 : 1 + span]
        total = total + row(2) * ahead[0:span]
        dup[0, b, pl.ds(at, span), :] = total.astype(jnp.bfloat16)

    @pl.loop(0, 2 * (steps - 1))
    def _(k):
        shift_rows(lax.rem(k, 2), k // 2)

    has_next = jnp.logical_or(y == 0, upper == 0)
    wait_dc = [copy("hd", (b,), m["halo_dc"].at[b], m["halo_dc"].at[b], across) for b in range(2)]
    wait_dc[0].wait_recv()
    pl.when(has_next)(wait_dc[1].wait_recv)
    dcv[0, rows : rows + 8, :] = m["halo_dc"][0]

    @pl.when(has_next)
    def _():
        dcv[1, rows : rows + 8, :] = m["halo_dc"][1]

    @pl.when(jnp.logical_not(has_next))
    def _():
        dcv[1, rows : rows + 8, :] = jnp.zeros((8, ca), jnp.float32)

    @pl.loop(0, 2)
    def _(b):
        shift_rows(b, steps - 1)

    def weight_grad(zz, yy):
        k = 2 * zz + yy
        return dot(abuf[0, 0, k], dup[0, 0], 1, 0) + dot(abuf[0, 1, k], dup[0, 1], 1, 0)

    def input_grad(b, k):
        return dot(wbuf[1, k], dup[0, b], 1, 1) + dot(wbuf[2, k], dup[1, b], 1, 1)

    b16, f32 = jnp.bfloat16, jnp.float32
    order = [far, zo, zp, z]
    ysend, yrecv, gown, zsend, zrecv = (m[k] for k in ("ysend", "yrecv", "gown", "zsend", "zrecv"))
    csend, crecv, pown, xsend, xrecv = (m[k] for k in ("csend", "crecv", "pown", "xsend", "xrecv"))
    psend, precv = m["psend"], m["precv"]
    gy, pc, px, pz = {}, {}, {}, {}

    def spot(bi, xi, half):
        return bi * 4 + xi * 2 + half

    def to_twin(bi, xi, half):
        b, xx, at = (1 - l, l)[bi], (1 - x, x)[xi], spot(bi, xi, half)
        csend[at] = input_grad(b, 2 * (xx * 2 + 1 - c) + half).astype(b16)
        pc[at] = push("pc", (at,), csend.at[at], crecv.at[at], twin)

    def keep(bi, xi, half):
        b, xx, at = (1 - l, l)[bi], (1 - x, x)[xi], spot(bi, xi, half)
        pown[at] = input_grad(b, 2 * (xx * 2 + c) + half)

    def to_x(bi, half):
        at, to = spot(bi, 0, half), bi * 2 + half
        pc[at].wait_recv()
        xsend[to] = (pown[at] + crecv[at].astype(f32)).astype(b16)
        px[to] = push("px", (to,), xsend.at[to], xrecv.at[to], x_dev)

    def to_pair(half):
        at = spot(0, 1, half)
        pc[at].wait_recv()
        px[half].wait_recv()
        total = pown[at] + crecv[at].astype(f32) + xrecv[half].astype(f32)
        psend[half] = total.astype(b16)
        pz[half] = push("pz", (half,), psend.at[half], precv.at[half], pair)

    def finish(half):
        at = spot(1, 1, half)
        pc[at].wait_recv()
        px[2 + half].wait_recv()
        pz[half].wait_recv()
        total = pown[at] + crecv[at].astype(f32)
        total = total + xrecv[2 + half].astype(f32) + precv[half].astype(f32)
        i_out[half] = total.astype(b16)

    for k in range(4):
        ysend[k] = weight_grad(order[k], 1 - y).astype(b16)
        gy[k] = push("gy", (k,), ysend.at[k], yrecv.at[k], across)
    for bi in range(2):
        for half in range(2):
            to_twin(bi, 0, half)
        for half in range(2):
            keep(bi, 0, half)
            to_x(bi, half)
    for k in range(4):
        gown[k] = weight_grad(order[k], y)

    def summed(k):
        gy[k].wait_recv()
        return gown[k] + yrecv[k].astype(f32)

    for k in range(3):
        c1[k].wait_recv()
    got = m["col_got"]
    m["col_sum"][...] = (m["col_own"][...] + got[0]) + (got[1] + got[2])
    place = m["col_all"].at[mine, 1 - inner_i]
    place[...] = m["col_sum"][...]
    c2 = []
    for k in range(1, 2 * t):
        tp = lax.rem(mine + k // 2, t)
        to = {"fs": (zp if k % 2 else z) * 2 + y, "tp": tp}
        c2.append(push("c2", (k - 1,), m["col_sum"], place, to))

    gz_wait = [copy("gz", (k,), zrecv.at[k], zrecv.at[k], across) for k in range(4)]
    zsend[0] = summed(0).astype(b16)
    first_to = inner_i * zo + (1 - inner_i) * far
    first_at = 3 - 2 * inner_i
    push("gz", (0,), zsend.at[0], zrecv.at[first_at], {"fs": first_to * 2 + y}, slot=(first_at,))
    zsend[1] = summed(1).astype(b16)
    push("gz", (1,), zsend.at[1], zrecv.at[0], {"fs": zo * 2 + y}, slot=(0,))
    for bi in range(2):
        for half in range(2):
            to_twin(bi, 1, half)
        for half in range(2):
            keep(bi, 1, half)
    to_pair(0)
    gown[2] = summed(2)

    @pl.when(outer)
    def _():
        zsend[2] = gown[2].astype(b16)

    @pl.when(inner)
    def _():
        gz_wait[1].wait_recv()
        zsend[2] = (gown[2] + zrecv[1].astype(f32)).astype(b16)

    last_at = 1 + (1 - inner_i)
    push("gz", (2,), zsend.at[2], zrecv.at[last_at], pair, slot=(last_at,))
    to_pair(1)
    gown[3] = summed(3)
    gz_wait[0].wait_recv()
    norm_own, norm_all = m["norm_own"], m["norm_all"]
    norm_own[...] = jnp.zeros(norm_own.shape, f32)

    def settle(k, value):
        g_out[:, k * ca : k * ca + (cb if k else ca)] = value[:, : (cb if k else ca)]
        norm_own[k : k + 1, :] = jnp.sum(value * value, axis=0, keepdims=True)

    @pl.when(inner)
    def _():
        settle(0, gown[3] + zrecv[0].astype(f32))
        gz_wait[2].wait_recv()
        gz_wait[3].wait_recv()
        settle(1, zrecv[2].astype(f32) + zrecv[3].astype(f32))

    @pl.when(outer)
    def _():
        settle(1, gown[3] + zrecv[0].astype(f32))
        gz_wait[1].wait_recv()
        settle(0, zrecv[1].astype(f32))

    norms = [
        push("nm", (k,), norm_own, norm_all.at[me], others[k]) for k in range(n - 1)
    ]
    finish(0)
    for copy_in in c2:
        copy_in.wait_recv()
    whole = m["col_all"]
    for p in range(t):
        at = p * width
        taps_out[:, at : at + ca] = whole[p, 0, 0:3, :]
        taps_out[:, at + ca : at + width] = whole[p, 1, 0:3, :cb]
        bias_out[:, at : at + ca] = whole[p, 0, 3:4, :]
        bias_out[:, at + ca : at + width] = whole[p, 1, 3:4, :cb]
    finish(1)
    for copy_in in norms:
        copy_in.wait_recv()
    norm_all[me] = norm_own[...]
    total = norm_all[0]
    for k in range(1, n):
        total = total + norm_all[k]
    norm_out[:, :ca] = total[0:1, :]
    norm_out[:, ca:] = total[1:2, :cb]
    for made in started:
        made.wait_send()
    pl.when(y == 0)(hu_near.wait_send)
    pl.when(jnp.logical_and(y == 1, upper == 0))(hu_far.wait_send)
    pl.when(y == 1)(hd_near.wait_send)
    pl.when(jnp.logical_and(y == 0, upper == 1))(hd_far.wait_send)


def with_kernel(inputs, w_conv_up, w_gate_up, w_down, taps, conv_bias, cotangent):
    n, t = lax.axis_size("fs"), lax.axis_size("tp")
    rows = inputs.shape[0]
    shard, width = w_conv_up.shape
    ca = -(-width // (2 * LANES)) * LANES
    shape = jax.ShapeDtypeStruct
    scratch = {**buffers(n, t, shard, rows, ca), **semaphores(n, t)}
    acts = [v.T.reshape(2, shard, rows) for v in (inputs, cotangent)]
    got = pl.pallas_call(
        functools.partial(layer_kernel, n, t, tuple(scratch)),
        out_shape=[
            shape((2, shard, rows), jnp.bfloat16),
            shape((shard, width), jnp.float32),
            shape((1, width), jnp.float32),
            shape((TAPS, t * width), jnp.float32),
            shape((1, t * width), jnp.float32),
        ],
        in_specs=[VMEM] * 7,
        out_specs=[VMEM] * 5,
        scratch_shapes=list(scratch.values()),
        compiler_params=pltpu.CompilerParams(
            collective_id=0, has_side_effects=True, vmem_limit_bytes=60 * 1024 * 1024
        ),
        name="layer",
    )(w_down.T, w_conv_up, w_gate_up, *acts, taps, conv_bias[None, :])
    grad_inputs, grad_conv_up, norms, grad_taps, grad_bias = got
    return (grad_inputs.reshape(-1, rows).T, grad_conv_up, norms[0], grad_taps, grad_bias[0])


def per_device(inputs, w_conv_up, *rest):
    n, t = lax.axis_size("fs"), lax.axis_size("tp")
    shard, width = w_conv_up.shape
    rows, features = inputs.shape
    fits = n == 8 and t == 4 and features == 2 * shard
    aligned = shard % 8 == 0 and rows % LANES == 0 and width > LANES
    chosen = with_kernel if fits and aligned else with_collectives
    return chosen(inputs, w_conv_up, *rest)


def solution(mesh):
    return jax.shard_map(
        per_device,
        mesh=mesh,
        in_specs=(
            P("fs", "tp"),
            P("fs", "tp"),
            P("fs", "tp"),
            P("tp", "fs"),
            P(),
            P(),
            P("fs", "tp"),
        ),
        out_specs=(P("fs", "tp"), P("fs", "tp"), P("tp"), P(), P()),
        check_vma=False,
    )
```

time: 188 us -> 144 us (0.77)
  Pallas kernels: 155 us -> 136 us
  matrix products: 12.7 us -> 0 us
  local copies, waits for them, and re-layouts: 9.17 us -> 4.71 us
  starting transfers between devices: 3.46 us -> 0 us
  other arithmetic: 6.1 us -> 2.68 us
    pallas_call x3 -> x1, Pallas kernels: 155 us -> 136 us  [with_kernel(): pl.pallas_call(functools.partial(layer_kernel, n, t, tuple(scratch)), out...]
    dot_general x6 -> x0, matrix products: 12.7 us -> none  [the longest x4 6.7 us: with_kernels(): lax.dot_general(weight[h], grad[:, slice(*starts[h])], (((1,), (1,)), (()...]
    slice x6 -> x0, local copies, waits for them, and re-layouts: 4.2 us -> none  [the longest x3 2.45 us: with_kernels(): return (grad_inputs.T, grad_conv_up, norms[0], full[:TAPS], full[TAPS])]
    ppermute x1 -> x0, starting transfers between devices: 3.46 us -> none  [shifted(): return lax.ppermute(block, axis, route)]
    convert_element_type x2 -> x0, other arithmetic: 2.42 us -> none  [the longest x1 1.3 us: with_kernels(): extended = jnp.concatenate([earlier, up_a], 0).astype(jnp.float32)]
  transfers between devices with their start and end apart: 1 -> 0, of which waited for: 0 -> 0; matrix products, arithmetic and copies ran while one was open for 1% -> 0% of each run, Pallas kernels for 0% -> 0%
where the time goes in v1:
time: 144 us
  Pallas kernels  136 us (94%)
  local copies, waits for them, and re-layouts  4.71 us (3%)
  other arithmetic  2.68 us (2%)
    pallas_call x1, Pallas kernels, with_kernel(): pl.pallas_call(functools.partial(layer_kernel, n, t, tuple(scratch)), out...  136 us
    unnamed x7, local copies, waits for them, and re-layouts  3.39 us

profile of v1, /device:TPU:0, one launch (start us, length us, event | category | flops | bytes accessed | tf_op | source)
XLA Modules:
  0.0 144.1 jit_solution(9208966282690191371)
XLA Ops:
  0.6 1.3 broadcast_in_dim.3.refs_6_
  1.9 136.1 %layer.1 = (bf16[2,264,512]{2,1,0:T(8,128)(2,1)}, f32[264,704]{1,0:T(8,128)}, f32[1,704]{1,0:T(1,128)}, f32[3,2816]{1,0:T(4,128)}, f32[1,2816]{1,0:T(1,128)}) custom-call(bf16[264,704]{1,0:T(8,128)(2,1)} %bitcast.13, bf16[264,704]{1,0:T(8,128)(2,1)} %refs_1_.1, bf16[264,704]{1,0:T(8,128)(2,1)} %refs_2_.1, bf16[2,264,512]{2,1,0:T(8,128)(2,1)} %bitcast.10, ...), custom_call_target="tpu_custom_call" | custom-call | tf_op jit(solution)/shard_map/layer/pallas_call | solution.py:594
  138.0 0.0 copy-start
  138.0 1.4 reduce.1
  139.5 1.3 reduce
  140.7 1.9 %copy.15 = bf16[512,528]{0,1:T(8,128)(2,1)} copy(bf16[512,528]{0,1:T(8,128)(2,1)} %bitcast.12) | data formatting | bytes 1081344
  142.6 0.0 copy-done
  142.6 0.0 copy-start.1
  142.6 0.9 copy.16
  143.5 0.0 copy-done.1
  143.5 0.6 copy.17
Async XLA Ops:
  138.0 4.6 %copy-start = (f32[264,704]{1,0:T(8,128)S(1)}, f32[264,704]{1,0:T(8,128)}, u32[]{:S(2)}) copy-start(f32[264,704]{1,0:T(8,128)} %get-tuple-element.21) | copy-start | bytes 2230276
  142.6 0.9 copy-start.1

commit v2 on v1

--- a/solution.py
+++ b/solution.py
@@ -11,7 +11,7 @@
 TAPS = 3
 LANES = 128
 MESH = pl.DeviceIdType.MESH
-VMEM = pl.BlockSpec(memory_space=pltpu.VMEM)
+VMEM_BYTES = 63 * 1024 * 1024
 ANY = pl.BlockSpec(memory_space=pl.ANY)
 
 
@@ -96,7 +96,10 @@
     barrier = pltpu.get_barrier_semaphore()
     for peer in peers:
         pl.semaphore_signal(barrier, inc=1, device_id=peer, device_id_type=MESH)
-    pl.semaphore_wait(barrier, len(peers))
+
+
+def greeted(peers):
+    pl.semaphore_wait(pltpu.get_barrier_semaphore(), len(peers))
 
 
 def dot(a, b, da, db):
@@ -109,10 +112,18 @@
     return value.astype(jnp.bfloat16).astype(jnp.float32)
 
 
-def buffers(n, t, shard, rows, ca):
+def buffers(n, t, shard, width, rows, ca):
     b16, f32 = jnp.bfloat16, jnp.float32
     return dict(
-        stage=pltpu.VMEM((3, shard, ca), b16),
+        wv=pltpu.VMEM((3, shard, width), b16),
+        taps_v=pltpu.VMEM((TAPS, t * width), f32),
+        bias_v=pltpu.VMEM((t * width,), f32),
+        i_v=pltpu.VMEM((2, shard, rows), b16),
+        g_v=pltpu.VMEM((shard, width), f32),
+        norm_v=pltpu.VMEM((width,), f32),
+        taps_w=pltpu.VMEM((TAPS, t * width), f32),
+        bias_w=pltpu.VMEM((t * width,), f32),
+        stage=pltpu.VMEM((2, 3, shard, ca), b16),
         wbuf=pltpu.VMEM((3, n, shard, ca), b16),
         abuf=pltpu.VMEM((2, 2, n, shard, rows), b16),
         tot=pltpu.VMEM((3, 2, rows + 8, ca), f32),
@@ -145,20 +156,22 @@
 def semaphores(n, t):
     shapes = dict(
         wz=(3, 3), wy=(3, 4), az=(4,), ax=(2, 4), ac=(4, 4), hu=(2,), hd=(2,),
-        c1=(3,), c2=(2 * t - 1,), gy=(4,), gz=(4,), pc=(8,), px=(4,), pz=(2,), nm=(n - 1,),
+        c1=(3,), c2=(2 * t - 1,), gy=(4, 2), gz=(4, 2), pc=(8,), px=(4,), pz=(2,), nm=(n - 1,),
     )
     dma = pltpu.SemaphoreType.DMA
-    return {name + end: dma(s) for name, s in shapes.items() for end in ("_s", "_r")}
+    local = dict(ld=dma((9,)), st=dma((6,)))
+    return local | {name + end: dma(s) for name, s in shapes.items() for end in ("_s", "_r")}
 
 
 def layer_kernel(n, t, names, *refs):
-    w, acts, taps, bias = refs[:3], refs[3:5], refs[5], refs[6]
-    i_out, g_out, norm_out, taps_out, bias_out = refs[7:12]
+    w_in, acts, taps_in, bias_in = refs[:3], refs[3:5], refs[5], refs[6]
+    outs = refs[7:12]
     m = dict(zip(names, refs[12:]))
     stage, wbuf, abuf, tot = m["stage"], m["wbuf"], m["abuf"], m["tot"]
     dcv, dup, tb = m["dcv"], m["dup"], m["tb"]
-    shard, width = w[0].shape
-    ca = stage.shape[2]
+    w, taps, bias = m["wv"], m["taps_v"], m["bias_v"]
+    shard, width = w.shape[1:]
+    ca = stage.shape[3]
     cb = width - ca
     rows = acts[0].shape[2]
     me, mine = lax.axis_index("fs"), lax.axis_index("tp")
@@ -177,7 +190,7 @@
     x_dev = {"tp": (1 - x) * 2 + c}
     twin = {"tp": x * 2 + 1 - c}
     x_tp = (1 - x) * 2 + c
-    line = [zp, far, zo]
+    line = [zp, 2 - upper, 3 * (1 - upper)]
     started = []
 
     def copy(name, at, src, dst, to, slot=None):
@@ -196,22 +209,38 @@
 
     def put(i, ref, first):
         if first:
-            ref[...] = w[i][:, :ca]
+            ref[...] = w[i, :, :ca]
         else:
             ref[:, cb // LANES * LANES :] = jnp.zeros(
                 (shard, ca - cb // LANES * LANES), jnp.bfloat16
             )
-            ref[:, :cb] = w[i][:, ca:]
+            ref[:, :cb] = w[i, :, ca:]
+
+    others = [{"fs": lax.rem(me + k, n)} for k in range(1, n)]
+    others += [{"tp": lax.rem(mine + k, t)} for k in range(1, t)]
+    others += [{"fs": zp * 2 + y, "tp": lax.rem(mine + k, t)} for k in range(1, t)]
+    greet(others)
+    loads = []
+
+    def load(src, dst):
+        made = pltpu.make_async_copy(src, dst, m["ld"].at[len(loads)])
+        made.start()
+        loads.append(made)
 
     for i in range(3):
-        for flag, first in ((inner, True), (outer, False)):
-            @pl.when(flag)
-            def _(i=i, first=first):
-                put(i, wbuf.at[i, me], first)
-                put(i, stage.at[i], not first)
+        load(w_in[i], w.at[i])
     for a in range(2):
         for half in range(2):
-            abuf[a, l, 2 * mine + half] = acts[a][half]
+            load(acts[a].at[half], abuf.at[a, l, 2 * mine + half])
+    load(taps_in, taps)
+    load(bias_in, bias)
+    for i in range(3):
+        loads[i].wait()
+        put(i, stage.at[0, i], True)
+        put(i, stage.at[1, i], False)
+        wbuf[i, me] = stage[1 - inner_i, i]
+    for made in loads[3:]:
+        made.wait()
     tb[...] = jnp.zeros(tb.shape, jnp.float32)
     for p in range(t):
         for flag, start, size in ((inner, 0, ca), (outer, ca, cb)):
@@ -219,12 +248,9 @@
             def _(p=p, start=start, size=size):
                 at = p * width + start
                 tb[0:3, 0:size] = taps[:, at : at + size]
-                tb[3:4, 0:size] = bias[:, at : at + size]
-
-    others = [{"fs": lax.rem(me + k, n)} for k in range(1, n)]
-    others += [{"tp": lax.rem(mine + k, t)} for k in range(1, t)]
-    others += [{"fs": zp * 2 + y, "tp": lax.rem(mine + k, t)} for k in range(1, t)]
-    greet(others)
+                tb[3:4, 0:size] = bias[at : at + size].reshape(1, size)
+
+    greeted(others)
 
     quarter = [(1, 0), (1, 1), (0, 0), (0, 1)]
     own_act = [abuf.at[a, l, 2 * mine + half] for a, half in quarter]
@@ -234,22 +260,22 @@
     az, ax, ac, wz, wy = {}, {}, {}, {}, {}
 
     def send_act(q):
-        a, half = quarter[q]
-        az[q] = push("az", (q,), acts[a].at[half], own_act[q], pair)
-        ax[0, q] = push("ax", (0, q), acts[a].at[half], own_act[q], x_dev)
-        ac[0, q] = push("ac", (0, q), acts[a].at[half], own_act[q], twin)
-
-    def send_w(i):
+        az[q] = push("az", (q,), own_act[q], own_act[q], pair)
+        ax[0, q] = push("ax", (0, q), own_act[q], own_act[q], x_dev)
+        ac[0, q] = push("ac", (0, q), own_act[q], own_act[q], twin)
+
+    def send_w(i, j):
         own = wbuf.at[i, me]
-        for j in range(3):
-            wz[i, j] = push(
-                "wz", (i, j), own if j == 2 else stage.at[i], own, {"fs": line[j] * 2 + y}
-            )
-        wy[i, 3] = push("wy", (i, 3), own, own, across)
+        if j == 3:
+            wy[i, 3] = push("wy", (i, 3), own, own, across)
+        else:
+            src = stage.at[inner_i if j == 0 else j - 1, i]
+            label = 0 if j == 0 else 2 - inner_i
+            push("wz", (i, j), src, own, {"fs": line[j] * 2 + y}, slot=(i, label))
 
     def pass_w(i, j):
-        wz[i, j].wait_recv()
         slot = wbuf.at[i, line[j] * 2 + y]
+        copy("wz", (i, j), slot, slot, pair).wait_recv()
         wy[i, j] = push("wy", (i, j), slot, slot, across)
 
     def pass_pair(q):
@@ -262,64 +288,53 @@
         ref = (x_act, xp_act)[way][q]
         ac[2 + way, q] = push("ac", (2 + way, q), ref, ref, twin)
 
-    def multiply(i, zz, fresh):
+    def multiply(i, zz, b, fresh):
         a = 1 if i == 0 else 0
-
-        @pl.loop(0, 2)
-        def _(b):
-            product = dot(abuf[a, b, 2 * zz], wbuf[i, 2 * zz], 0, 0)
-            product = product + dot(abuf[a, b, 2 * zz + 1], wbuf[i, 2 * zz + 1], 0, 0)
-            if fresh:
-                tot[i, b, 8:, :] = product
-            else:
-                tot[i, b, 8:, :] = tot[i, b, 8:, :] + product
-
-    send_act(0)
-    send_act(1)
-    send_w(0)
-    send_act(2)
-    send_w(1)
-    send_act(3)
-    send_w(2)
-    pass_pair(0)
-    pass_x(0, 0)
-    pass_x(0, 1)
-    pass_pair(1)
-    for j in range(3):
-        pass_w(0, j)
-    pass_x(0, 2)
-    pass_x(0, 3)
-    pass_x(1, 0)
-    pass_pair(2)
-    pass_x(1, 1)
-    for j in range(3):
-        pass_w(1, j)
-    pass_pair(3)
-    pass_x(1, 2)
-    for s in range(4):
-        for q in range(2):
-            ac[s, q].wait_recv()
-    for k, j in enumerate((3, 0, 1, 2)):
-        wy[0, j].wait_recv()
-        multiply(0, z if j == 3 else line[j], k == 0)
-    pass_x(1, 3)
-    for s in range(4):
-        for q in range(2, 4):
-            ac[s, q].wait_recv()
-    for k, j in enumerate((3, 0, 1, 2)):
-        wy[1, j].wait_recv()
-        multiply(1, z if j == 3 else line[j], k == 0)
+        product = dot(abuf[a, b, 2 * zz], wbuf[i, 2 * zz], 0, 0)
+        product = product + dot(abuf[a, b, 2 * zz + 1], wbuf[i, 2 * zz + 1], 0, 0)
+        if fresh:
+            tot[i, b, 8:, :] = product
+        else:
+            tot[i, b, 8:, :] = tot[i, b, 8:, :] + product
+
+    arrived, acts_seen = set(), set()
+
+    def compute(i, j, which):
+        if (i, j) not in arrived:
+            arrived.add((i, j))
+            wy[i, j].wait_recv()
+        for q in (0, 1) if i == 0 else (2, 3):
+            for s in (0, 2) if which == 0 else (1, 3):
+                if (s, q) not in acts_seen:
+                    acts_seen.add((s, q))
+                    ac[s, q].wait_recv()
+        multiply(i, z if j == 3 else line[j], l if which == 0 else 1 - l, j == 3)
+
+    sending = (
+        "a0 a1 w03 w02", "w01 w13 a2 w00", "w12 w11 w23 a3", "w22 w21 w10 w20",
+    )
+    for item in " ".join(sending).split():
+        if item[0] == "a":
+            send_act(int(item[1]))
+        else:
+            send_w(int(item[1]), int(item[2]))
+    passing = (
+        "x00 w01 p0", "x01 c030 x02 w02", "p1 c010 x03 w11", "c130 c230 x10 p2",
+        "c020 w12 x11 c110", "c031 w00 c011 w21", "x12 c120 c021 p3", "w22 c000 c001 w10",
+        "c210 x13 c220 c131", "c111 w20 c121 c100", "c101",
+    )
+    for item in " ".join(passing).split():
+        at = [int(v) for v in item[1:]]
+        dict(x=pass_x, w=pass_w, p=pass_pair, c=compute)[item[0]](*at)
     for b in range(2):
         edge, where = tot.at[1, b, pl.ds(rows, 8)], m["halo_up"]
         if b == 0:
-            hu0 = push("hu", (0,), edge, where.at[y], across, slot=(y,))
+            push("hu", (0,), edge, where.at[y], across, slot=(y,))
         else:
             hu_near = copy("hu", (1,), edge, where.at[1], across)
             hu_far = copy("hu", (1,), edge, where.at[0], {"fs": zo * 2}, slot=(0,))
             pl.when(y == 0)(hu_near.start)
             pl.when(jnp.logical_and(y == 1, upper == 0))(hu_far.start)
-    for j in range(3):
-        pass_w(2, j)
 
     span = 32
     steps = rows // span
@@ -342,9 +357,9 @@
     def _(k):
         gelu_rows(lax.rem(k, 2), 1 + k // 2)
 
+    for j in (3, 1, 2):
+        compute(2, j, 1)
     has_before = jnp.logical_or(y == 1, upper == 1)
-    has_after = jnp.logical_or(y == 1 - 0, y == 0)
-    del has_after
     wait_up = [copy("hu", (b,), m["halo_up"].at[b], m["halo_up"].at[b], across) for b in range(2)]
     wait_up[1].wait_recv()
     pl.when(has_before)(wait_up[0].wait_recv)
@@ -362,9 +377,8 @@
     def _(b):
         gelu_rows(b, 0)
 
-    for k, j in enumerate((3, 0, 1, 2)):
-        wy[2, j].wait_recv()
-        multiply(2, z if j == 3 else line[j], k == 0)
+    for which in range(2):
+        compute(2, 0, which)
 
     def grad_rows(b, r, sums):
         at = pl.multiple_of(r * span, span)
@@ -467,6 +481,16 @@
         psend[half] = total.astype(b16)
         pz[half] = push("pz", (half,), psend.at[half], precv.at[half], pair)
 
+    i_v, g_v, norm_v, taps_w, bias_w = (
+        m[k] for k in ("i_v", "g_v", "norm_v", "taps_w", "bias_w")
+    )
+    stores = []
+
+    def store(src, dst):
+        made = pltpu.make_async_copy(src, dst, m["st"].at[len(stores)])
+        made.start()
+        stores.append(made)
+
     def finish(half):
         at = spot(1, 1, half)
         pc[at].wait_recv()
@@ -474,98 +498,143 @@
         pz[half].wait_recv()
         total = pown[at] + crecv[at].astype(f32)
         total = total + xrecv[2 + half].astype(f32) + precv[half].astype(f32)
-        i_out[half] = total.astype(b16)
-
-    for k in range(4):
-        ysend[k] = weight_grad(order[k], 1 - y).astype(b16)
-        gy[k] = push("gy", (k,), ysend.at[k], yrecv.at[k], across)
-    for bi in range(2):
-        for half in range(2):
-            to_twin(bi, 0, half)
-        for half in range(2):
-            keep(bi, 0, half)
-            to_x(bi, half)
-    for k in range(4):
-        gown[k] = weight_grad(order[k], y)
-
-    def summed(k):
-        gy[k].wait_recv()
-        return gown[k] + yrecv[k].astype(f32)
-
-    for k in range(3):
-        c1[k].wait_recv()
-    got = m["col_got"]
-    m["col_sum"][...] = (m["col_own"][...] + got[0]) + (got[1] + got[2])
-    place = m["col_all"].at[mine, 1 - inner_i]
-    place[...] = m["col_sum"][...]
-    c2 = []
-    for k in range(1, 2 * t):
-        tp = lax.rem(mine + k // 2, t)
-        to = {"fs": (zp if k % 2 else z) * 2 + y, "tp": tp}
-        c2.append(push("c2", (k - 1,), m["col_sum"], place, to))
-
-    gz_wait = [copy("gz", (k,), zrecv.at[k], zrecv.at[k], across) for k in range(4)]
-    zsend[0] = summed(0).astype(b16)
+        i_v[half] = total.astype(b16)
+        store(i_v.at[half], outs[0].at[half])
+
+    first_rows = -(-shard // 16) * 8
+    parts = (pl.ds(0, first_rows), pl.ds(first_rows, shard - first_rows))
     first_to = inner_i * zo + (1 - inner_i) * far
     first_at = 3 - 2 * inner_i
-    push("gz", (0,), zsend.at[0], zrecv.at[first_at], {"fs": first_to * 2 + y}, slot=(first_at,))
-    zsend[1] = summed(1).astype(b16)
-    push("gz", (1,), zsend.at[1], zrecv.at[0], {"fs": zo * 2 + y}, slot=(0,))
-    for bi in range(2):
-        for half in range(2):
-            to_twin(bi, 1, half)
-        for half in range(2):
-            keep(bi, 1, half)
+    last_at = 2 - inner_i
+
+    def to_across(k):
+        ysend[k] = weight_grad(order[k], 1 - y).astype(b16)
+        for s, at in enumerate(parts):
+            gy[k, s] = push("gy", (k, s), ysend.at[k, at], yrecv.at[k, at], across)
+
+    def own(k):
+        gown[k] = weight_grad(order[k], y)
+
+    def add_across(k, s):
+        gy[k, s].wait_recv()
+        at = parts[s]
+        gown[k, at, :] = gown[k, at, :] + yrecv[k, at, :].astype(f32)
+
+    def to_line(k, s, dev, slot):
+        at = parts[s]
+        push(
+            "gz", (k, s), zsend.at[k, at], zrecv.at[slot, at], {"fs": dev * 2 + y}, slot=(slot, s)
+        )
+
+    def got_line(k, s):
+        at = parts[s]
+        copy("gz", (k, s), zrecv.at[k, at], zrecv.at[k, at], across).wait_recv()
+
+    def send_columns():
+        for k in range(3):
+            c1[k].wait_recv()
+        got = m["col_got"]
+        m["col_sum"][...] = (m["col_own"][...] + got[0]) + (got[1] + got[2])
+        place = m["col_all"].at[mine, 1 - inner_i]
+        place[...] = m["col_sum"][...]
+        for k in range(1, 2 * t):
+            tp = lax.rem(mine + k // 2, t)
+            to = {"fs": (zp if k % 2 else z) * 2 + y, "tp": tp}
+            c2.append(push("c2", (k - 1,), m["col_sum"], place, to))
+
+    c2 = []
+    to_across(0)
+    to_twin(0, 0, 0)
+    to_across(1)
+    to_twin(0, 0, 1)
+    keep(0, 0, 0)
+    send_columns()
+    to_x(0, 0)
+    keep(0, 0, 1)
+    to_x(0, 1)
+    to_across(2)
+    to_across(3)
+    own(0)
+    for s in range(2):
+        add_across(0, s)
+        zsend[0, parts[s], :] = gown[0, parts[s], :].astype(b16)
+        to_line(0, s, first_to, first_at)
+    own(1)
+    to_twin(1, 0, 0)
+    to_twin(1, 0, 1)
+    keep(1, 0, 0)
+    to_x(1, 0)
+    for s in range(2):
+        add_across(1, s)
+        zsend[1, parts[s], :] = gown[1, parts[s], :].astype(b16)
+        to_line(1, s, zo, 0)
+    keep(1, 0, 1)
+    to_x(1, 1)
+    own(2)
+    to_twin(0, 1, 0)
+    to_twin(0, 1, 1)
+    keep(0, 1, 0)
+    keep(0, 1, 1)
+    for s in range(2):
+        add_across(2, s)
+
+        @pl.when(outer)
+        def _(at=parts[s]):
+            zsend[2, at, :] = gown[2, at, :].astype(b16)
+
+        @pl.when(inner)
+        def _(s=s, at=parts[s]):
+            got_line(1, s)
+            zsend[2, at, :] = (gown[2, at, :] + zrecv[1, at, :].astype(f32)).astype(b16)
+
+        to_line(2, s, zp, last_at)
     to_pair(0)
-    gown[2] = summed(2)
-
-    @pl.when(outer)
-    def _():
-        zsend[2] = gown[2].astype(b16)
-
-    @pl.when(inner)
-    def _():
-        gz_wait[1].wait_recv()
-        zsend[2] = (gown[2] + zrecv[1].astype(f32)).astype(b16)
-
-    last_at = 1 + (1 - inner_i)
-    push("gz", (2,), zsend.at[2], zrecv.at[last_at], pair, slot=(last_at,))
-    to_pair(1)
-    gown[3] = summed(3)
-    gz_wait[0].wait_recv()
+    own(3)
+    for half in range(2):
+        to_twin(1, 1, half)
+        keep(1, 1, half)
+    for s in range(2):
+        add_across(3, s)
+        got_line(0, s)
     norm_own, norm_all = m["norm_own"], m["norm_all"]
     norm_own[...] = jnp.zeros(norm_own.shape, f32)
 
     def settle(k, value):
-        g_out[:, k * ca : k * ca + (cb if k else ca)] = value[:, : (cb if k else ca)]
+        g_v[:, k * ca : k * ca + (cb if k else ca)] = value[:, : (cb if k else ca)]
         norm_own[k : k + 1, :] = jnp.sum(value * value, axis=0, keepdims=True)
 
     @pl.when(inner)
     def _():
         settle(0, gown[3] + zrecv[0].astype(f32))
-        gz_wait[2].wait_recv()
-        gz_wait[3].wait_recv()
+        for s in range(2):
+            got_line(2, s)
+            got_line(3, s)
         settle(1, zrecv[2].astype(f32) + zrecv[3].astype(f32))
 
     @pl.when(outer)
     def _():
         settle(1, gown[3] + zrecv[0].astype(f32))
-        gz_wait[1].wait_recv()
+        for s in range(2):
+            got_line(1, s)
         settle(0, zrecv[1].astype(f32))
 
     norms = [
         push("nm", (k,), norm_own, norm_all.at[me], others[k]) for k in range(n - 1)
     ]
+    to_pair(1)
+    store(g_v, outs[1])
     finish(0)
     for copy_in in c2:
         copy_in.wait_recv()
     whole = m["col_all"]
     for p in range(t):
         at = p * width
-        taps_out[:, at : at + ca] = whole[p, 0, 0:3, :]
-        taps_out[:, at + ca : at + width] = whole[p, 1, 0:3, :cb]
-        bias_out[:, at : at + ca] = whole[p, 0, 3:4, :]
-        bias_out[:, at + ca : at + width] = whole[p, 1, 3:4, :cb]
+        taps_w[:, at : at + ca] = whole[p, 0, 0:3, :]
+        taps_w[:, at + ca : at + width] = whole[p, 1, 0:3, :cb]
+        bias_w[at : at + ca] = whole[p, 0, 3, :]
+        bias_w[at + ca : at + width] = whole[p, 1, 3, :cb]
+    store(taps_w, outs[3])
+    store(bias_w, outs[4])
     finish(1)
     for copy_in in norms:
         copy_in.wait_recv()
@@ -573,14 +642,44 @@
     total = norm_all[0]
     for k in range(1, n):
         total = total + norm_all[k]
-    norm_out[:, :ca] = total[0:1, :]
-    norm_out[:, ca:] = total[1:2, :cb]
+    norm_v[:ca] = total[0]
+    norm_v[ca:] = total[1, :cb]
+    store(norm_v, outs[2])
     for made in started:
         made.wait_send()
+    for made in stores:
+        made.wait()
     pl.when(y == 0)(hu_near.wait_send)
     pl.when(jnp.logical_and(y == 1, upper == 0))(hu_far.wait_send)
     pl.when(y == 1)(hd_near.wait_send)
     pl.when(jnp.logical_and(y == 0, upper == 1))(hd_far.wait_send)
+
+
+def publish_kernel(n, *refs):
+    src, dst, held, sem = refs[:n], refs[n : 2 * n], refs[2 * n : 3 * n], refs[3 * n]
+    into = [pltpu.make_async_copy(src[k], held[k], sem.at[0, k]) for k in range(n)]
+    out = [pltpu.make_async_copy(held[k], dst[k], sem.at[1, k]) for k in range(n)]
+    for made in into:
+        made.start()
+    for k in range(n):
+        into[k].wait()
+        out[k].start()
+    for made in out:
+        made.wait()
+
+
+def publish(*arrays):
+    n = len(arrays)
+    return pl.pallas_call(
+        functools.partial(publish_kernel, n),
+        out_shape=[jax.ShapeDtypeStruct(v.shape, v.dtype) for v in arrays],
+        in_specs=[ANY] * n,
+        out_specs=[ANY] * n,
+        scratch_shapes=[pltpu.VMEM(v.shape, v.dtype) for v in arrays]
+        + [pltpu.SemaphoreType.DMA((2, n))],
+        compiler_params=pltpu.CompilerParams(vmem_limit_bytes=VMEM_BYTES),
+        name="publish",
+    )(*arrays)
 
 
 def with_kernel(inputs, w_conv_up, w_gate_up, w_down, taps, conv_bias, cotangent):
@@ -589,27 +688,27 @@
     shard, width = w_conv_up.shape
     ca = -(-width // (2 * LANES)) * LANES
     shape = jax.ShapeDtypeStruct
-    scratch = {**buffers(n, t, shard, rows, ca), **semaphores(n, t)}
+    scratch = {**buffers(n, t, shard, width, rows, ca), **semaphores(n, t)}
     acts = [v.T.reshape(2, shard, rows) for v in (inputs, cotangent)]
     got = pl.pallas_call(
         functools.partial(layer_kernel, n, t, tuple(scratch)),
         out_shape=[
             shape((2, shard, rows), jnp.bfloat16),
             shape((shard, width), jnp.float32),
-            shape((1, width), jnp.float32),
+            shape((width,), jnp.float32),
             shape((TAPS, t * width), jnp.float32),
-            shape((1, t * width), jnp.float32),
+            shape((t * width,), jnp.float32),
         ],
-        in_specs=[VMEM] * 7,
-        out_specs=[VMEM] * 5,
+        in_specs=[ANY] * 7,
+        out_specs=[ANY] * 5,
         scratch_shapes=list(scratch.values()),
         compiler_params=pltpu.CompilerParams(
-            collective_id=0, has_side_effects=True, vmem_limit_bytes=60 * 1024 * 1024
+            collective_id=0, has_side_effects=True, vmem_limit_bytes=VMEM_BYTES
         ),
         name="layer",
-    )(w_down.T, w_conv_up, w_gate_up, *acts, taps, conv_bias[None, :])
-    grad_inputs, grad_conv_up, norms, grad_taps, grad_bias = got
-    return (grad_inputs.reshape(-1, rows).T, grad_conv_up, norms[0], grad_taps, grad_bias[0])
+    )(w_down.T, w_conv_up, w_gate_up, *acts, taps, conv_bias)
+    grad_inputs, *others = publish(*got)
+    return (grad_inputs.reshape(-1, rows).T, *others)
 
 
 def per_device(inputs, w_conv_up, *rest):

time: 144 us -> 125 us (0.87)
  Pallas kernels: 136 us -> 124 us
  local copies, waits for them, and re-layouts: 4.71 us -> 0 us
  other arithmetic: 2.68 us -> 0 us
    pallas_call x1, Pallas kernels: 136 us -> 122 us  [with_kernel(): pl.pallas_call(functools.partial(layer_kernel, n, t, tuple(scratch)), out...]
    unnamed x7 -> x0, local copies, waits for them, and re-layouts: 3.39 us -> none
    pallas_call x2 -> x0, other arithmetic: 2.68 us -> none  [with_kernel(): pl.pallas_call(functools.partial(layer_kernel, n, t, tuple(scratch)), out...]
    pallas_call x0 -> x1, Pallas kernels: none -> 2.29 us  [publish(): pl.pallas_call(functools.partial(publish_kernel, n), out_shape=[jax.Shape...]
where the time goes in v2:
time: 125 us
  Pallas kernels  124 us (99%)
    pallas_call x1, Pallas kernels, with_kernel(): pl.pallas_call(functools.partial(layer_kernel, n, t, tuple(scratch)), out...  122 us

profile of v2, /device:TPU:0, one launch (start us, length us, event | category | flops | bytes accessed | tf_op | source)
XLA Modules:
  0.0 125.0 jit_solution(10110116561867049421)
XLA Ops:
  0.6 121.9 %layer.1 = (bf16[2,264,512]{2,1,0:T(8,128)(2,1)}, f32[264,704]{1,0:T(8,128)}, f32[704]{0:T(1024)}, f32[3,2816]{1,0:T(4,128)}, f32[2816]{0:T(1024)}) custom-call(bf16[264,704]{1,0:T(8,128)(2,1)} %bitcast.12, bf16[264,704]{1,0:T(8,128)(2,1)} %refs_1_.1, bf16[264,704]{1,0:T(8,128)(2,1)} %refs_2_.1, bf16[2,264,512]{2,1,0:T(8,128)(2,1)} %bitcast.10, ...), custom_call_target="tpu_custom_call" | custom-call | tf_op jit(solution)/shard_map/layer/pallas_call | solution.py:693
  122.6 2.3 %publish.1 = (bf16[2,264,512]{2,1,0:T(8,128)(2,1)}, f32[264,704]{1,0:T(8,128)}, f32[704]{0:T(1024)}, f32[3,2816]{1,0:T(4,128)}, f32[2816]{0:T(1024)}) custom-call(bf16[2,264,512]{2,1,0:T(8,128)(2,1)} %get-tuple-element.15.refs_0_, f32[264,704]{1,0:T(8,128)} %get-tuple-element.16.refs_1_, f32[704]{0:T(1024)} %get-tuple-element.17.refs_2_, ...), custom_call_target="tpu_custom_call" | custom-call | tf_op jit(solution)/shard_map/publish/pallas_call | solution.py:673

commit v3 on v2

--- a/solution.py
+++ b/solution.py
@@ -112,8 +112,13 @@
     return value.astype(jnp.bfloat16).astype(jnp.float32)
 
 
+def folded_rows(rows):
+    return -(-rows // 32) * 16
+
+
 def buffers(n, t, shard, width, rows, ca):
     b16, f32 = jnp.bfloat16, jnp.float32
+    full, fold = ca // LANES - 1, folded_rows(shard)
     return dict(
         wv=pltpu.VMEM((3, shard, width), b16),
         taps_v=pltpu.VMEM((TAPS, t * width), f32),
@@ -123,8 +128,12 @@
         norm_v=pltpu.VMEM((width,), f32),
         taps_w=pltpu.VMEM((TAPS, t * width), f32),
         bias_w=pltpu.VMEM((t * width,), f32),
-        stage=pltpu.VMEM((2, 3, shard, ca), b16),
-        wbuf=pltpu.VMEM((3, n, shard, ca), b16),
+        stage=pltpu.VMEM((2, 3, full, shard, LANES), b16),
+        stage_end=pltpu.VMEM((3, shard, LANES), b16),
+        stage_fold=pltpu.VMEM((3, fold, LANES), b16),
+        wmain=pltpu.VMEM((3, n, full, shard, LANES), b16),
+        wend=pltpu.VMEM((3, n, shard, LANES), b16),
+        wfold=pltpu.VMEM((3, n, fold, LANES), b16),
         abuf=pltpu.VMEM((2, 2, n, shard, rows), b16),
         tot=pltpu.VMEM((3, 2, rows + 8, ca), f32),
         halo_up=pltpu.VMEM((2, 8, ca), f32),
@@ -155,7 +164,7 @@
 
 def semaphores(n, t):
     shapes = dict(
-        wz=(3, 3), wy=(3, 4), az=(4,), ax=(2, 4), ac=(4, 4), hu=(2,), hd=(2,),
+        wz=(3, 3), wy=(3, 4), ez=(3, 3), ey=(3, 4), az=(4,), ax=(2, 4), ac=(4, 4), hu=(2,), hd=(2,),
         c1=(3,), c2=(2 * t - 1,), gy=(4, 2), gz=(4, 2), pc=(8,), px=(4,), pz=(2,), nm=(n - 1,),
     )
     dma = pltpu.SemaphoreType.DMA
@@ -167,12 +176,15 @@
     w_in, acts, taps_in, bias_in = refs[:3], refs[3:5], refs[5], refs[6]
     outs = refs[7:12]
     m = dict(zip(names, refs[12:]))
-    stage, wbuf, abuf, tot = m["stage"], m["wbuf"], m["abuf"], m["tot"]
+    stage, stage_end, stage_fold = m["stage"], m["stage_end"], m["stage_fold"]
+    wmain, wend, wfold, abuf, tot = m["wmain"], m["wend"], m["wfold"], m["abuf"], m["tot"]
     dcv, dup, tb = m["dcv"], m["dup"], m["tb"]
     w, taps, bias = m["wv"], m["taps_v"], m["bias_v"]
     shard, width = w.shape[1:]
-    ca = stage.shape[3]
+    full, fold = stage.shape[2], stage_fold.shape[1]
+    ca = (full + 1) * LANES
     cb = width - ca
+    odd = cb - full * LANES
     rows = acts[0].shape[2]
     me, mine = lax.axis_index("fs"), lax.axis_index("tp")
     z, y = me // 2, lax.rem(me, 2)
@@ -191,7 +203,7 @@
     twin = {"tp": x * 2 + 1 - c}
     x_tp = (1 - x) * 2 + c
     line = [zp, 2 - upper, 3 * (1 - upper)]
-    started = []
+    started, guarded = [], []
 
     def copy(name, at, src, dst, to, slot=None):
         slot = at if slot is None else slot
@@ -207,14 +219,42 @@
         started.append(made)
         return made
 
-    def put(i, ref, first):
-        if first:
-            ref[...] = w[i, :, :ca]
-        else:
-            ref[:, cb // LANES * LANES :] = jnp.zeros(
-                (shard, ca - cb // LANES * LANES), jnp.bfloat16
-            )
-            ref[:, :cb] = w[i, :, ca:]
+    def push_if(flag, *args, **kw):
+        made = copy(*args, **kw)
+        pl.when(flag)(made.start)
+        guarded.append((flag, made))
+
+    def put(i):
+        for k in range(full):
+            at = k * LANES
+            stage[0, i, k] = w[i, :, at : at + LANES]
+            stage[1, i, k] = w[i, :, ca + at : ca + at + LANES]
+        end = w[i, :, ca + full * LANES :]
+        stage_end[i] = w[i, :, full * LANES : ca]
+        stage_fold[i] = jnp.zeros((fold, LANES), jnp.bfloat16)
+        stage_fold[i, :, :odd] = end[:fold]
+        stage_fold[i, : shard - fold, odd:] = end[fold:]
+        wmain[i, me] = stage[1 - inner_i, i]
+
+        @pl.when(inner)
+        def _():
+            wend[i, me] = stage_end[i]
+
+        @pl.when(outer)
+        def _():
+            wend[i, me] = jnp.zeros((shard, LANES), jnp.bfloat16)
+            wend[i, me, :, :odd] = end
+
+    def unfold(i, k):
+        both = wfold[i, k].astype(jnp.float32)
+        low = lax.broadcasted_iota(jnp.int32, both.shape, 1) < odd
+        first = jnp.where(low, both, 0.0).astype(jnp.bfloat16)
+        second = jnp.where(low, pltpu.roll(both, LANES - odd, 1), 0.0).astype(jnp.bfloat16)
+        wend[i, k, :fold] = first
+        wend[i, k, fold:] = second[: shard - fold]
+
+    def weight(i, k):
+        return jnp.concatenate([wmain[i, k, c] for c in range(full)] + [wend[i, k]], axis=1)
 
     others = [{"fs": lax.rem(me + k, n)} for k in range(1, n)]
     others += [{"tp": lax.rem(mine + k, t)} for k in range(1, t)]
@@ -236,9 +276,7 @@
     load(bias_in, bias)
     for i in range(3):
         loads[i].wait()
-        put(i, stage.at[0, i], True)
-        put(i, stage.at[1, i], False)
-        wbuf[i, me] = stage[1 - inner_i, i]
+        put(i)
     for made in loads[3:]:
         made.wait()
     tb[...] = jnp.zeros(tb.shape, jnp.float32)
@@ -265,18 +303,32 @@
         ac[0, q] = push("ac", (0, q), own_act[q], own_act[q], twin)
 
     def send_w(i, j):
-        own = wbuf.at[i, me]
+        own, own_end, own_fold = wmain.at[i, me], wend.at[i, me], wfold.at[i, me]
+        ends, folds = stage_end.at[i], stage_fold.at[i]
         if j == 3:
             wy[i, 3] = push("wy", (i, 3), own, own, across)
+            push_if(inner, "ey", (i, 3), ends, own_end, across)
+            push_if(outer, "ey", (i, 3), folds, own_fold, across)
+            return
+        to = {"fs": line[j] * 2 + y}
+        at = (i, 0 if j == 0 else 2 - inner_i)
+        push("wz", (i, j), stage.at[inner_i if j == 0 else j - 1, i], own, to, slot=at)
+        if j == 0:
+            push_if(outer, "ez", (i, j), ends, own_end, to, slot=at)
+            push_if(inner, "ez", (i, j), folds, own_fold, to, slot=at)
+        elif j == 1:
+            push("ez", (i, j), ends, own_end, to, slot=at)
         else:
-            src = stage.at[inner_i if j == 0 else j - 1, i]
-            label = 0 if j == 0 else 2 - inner_i
-            push("wz", (i, j), src, own, {"fs": line[j] * 2 + y}, slot=(i, label))
+            push("ez", (i, j), folds, own_fold, to, slot=at)
 
     def pass_w(i, j):
-        slot = wbuf.at[i, line[j] * 2 + y]
+        k = line[j] * 2 + y
+        slot = wmain.at[i, k]
         copy("wz", (i, j), slot, slot, pair).wait_recv()
         wy[i, j] = push("wy", (i, j), slot, slot, across)
+        for flag, ref in ((inner, wend.at[i, k]), (outer, wfold.at[i, k])):
+            pl.when(flag)(copy("ez", (i, j), ref, ref, pair).wait_recv)
+            push_if(flag, "ey", (i, j), ref, ref, across)
 
     def pass_pair(q):
         az[q].wait_recv()
@@ -288,10 +340,12 @@
         ref = (x_act, xp_act)[way][q]
         ac[2 + way, q] = push("ac", (2 + way, q), ref, ref, twin)
 
-    def multiply(i, zz, b, fresh):
+    def multiply(i, zz, b, halves, fresh):
         a = 1 if i == 0 else 0
-        product = dot(abuf[a, b, 2 * zz], wbuf[i, 2 * zz], 0, 0)
-        product = product + dot(abuf[a, b, 2 * zz + 1], wbuf[i, 2 * zz + 1], 0, 0)
+        product = 0.0
+        for half in halves:
+            k = 2 * zz + half
+            product = product + dot(abuf[a, b, k], weight(i, k), 0, 0)
         if fresh:
             tot[i, b, 8:, :] = product
         else:
@@ -299,16 +353,32 @@
 
     arrived, acts_seen = set(), set()
 
-    def compute(i, j, which):
+    def compute(i, j, which, *only):
+        halves = only or (0, 1)
         if (i, j) not in arrived:
             arrived.add((i, j))
             wy[i, j].wait_recv()
-        for q in (0, 1) if i == 0 else (2, 3):
+            zz = z if j == 3 else line[j]
+            k = zz * 2 + 1 - y
+
+            @pl.when(inner)
+            def _():
+                copy("ey", (i, j), wend.at[i, k], wend.at[i, k], across).wait_recv()
+
+            @pl.when(outer)
+            def _():
+                copy("ey", (i, j), wfold.at[i, k], wfold.at[i, k], across).wait_recv()
+                unfold(i, k)
+                if j != 3:
+                    unfold(i, zz * 2 + y)
+
+        for q in [half + (2 if i else 0) for half in halves]:
             for s in (0, 2) if which == 0 else (1, 3):
                 if (s, q) not in acts_seen:
                     acts_seen.add((s, q))
                     ac[s, q].wait_recv()
-        multiply(i, z if j == 3 else line[j], l if which == 0 else 1 - l, j == 3)
+        fresh = j == 3 and halves[0] == 0
+        multiply(i, z if j == 3 else line[j], l if which == 0 else 1 - l, halves, fresh)
 
     sending = (
         "a0 a1 w03 w02", "w01 w13 a2 w00", "w12 w11 w23 a3", "w22 w21 w10 w20",
@@ -319,9 +389,9 @@
         else:
             send_w(int(item[1]), int(item[2]))
     passing = (
-        "x00 w01 p0", "x01 c030 x02 w02", "p1 c010 x03 w11", "c130 c230 x10 p2",
-        "c020 w12 x11 c110", "c031 w00 c011 w21", "x12 c120 c021 p3", "w22 c000 c001 w10",
-        "c210 x13 c220 c131", "c111 w20 c121 c100", "c101",
+        "x00 w01 p0 x01", "c030 x02 w02 p1", "c010 x03 w11 c130", "c230 x10 p2 c020",
+        "w12 x11 c110 c031", "w00 c011 w21 x12", "c120 c021 c1310 c1110", "p3 w22 c2310 c1210",
+        "c000 c001 w10 c210", "c2110 x13 c220 c1311", "c1111 w20 c1211 c100", "c101",
     )
     for item in " ".join(passing).split():
         at = [int(v) for v in item[1:]]
@@ -357,8 +427,9 @@
     def _(k):
         gelu_rows(lax.rem(k, 2), 1 + k // 2)
 
-    for j in (3, 1, 2):
-        compute(2, j, 1)
+    compute(2, 3, 1, 1)
+    compute(2, 1, 1, 1)
+    compute(2, 2, 1)
     has_before = jnp.logical_or(y == 1, upper == 1)
     wait_up = [copy("hu", (b,), m["halo_up"].at[b], m["halo_up"].at[b], across) for b in range(2)]
     wait_up[1].wait_recv()
@@ -446,7 +517,7 @@
         return dot(abuf[0, 0, k], dup[0, 0], 1, 0) + dot(abuf[0, 1, k], dup[0, 1], 1, 0)
 
     def input_grad(b, k):
-        return dot(wbuf[1, k], dup[0, b], 1, 1) + dot(wbuf[2, k], dup[1, b], 1, 1)
+        return dot(weight(1, k), dup[0, b], 1, 1) + dot(weight(2, k), dup[1, b], 1, 1)
 
     b16, f32 = jnp.bfloat16, jnp.float32
     order = [far, zo, zp, z]
@@ -575,6 +646,7 @@
     to_twin(0, 1, 1)
     keep(0, 1, 0)
     keep(0, 1, 1)
+    to_pair(0)
     for s in range(2):
         add_across(2, s)
 
@@ -588,7 +660,7 @@
             zsend[2, at, :] = (gown[2, at, :] + zrecv[1, at, :].astype(f32)).astype(b16)
 
         to_line(2, s, zp, last_at)
-    to_pair(0)
+    to_pair(1)
     own(3)
     for half in range(2):
         to_twin(1, 1, half)
@@ -621,7 +693,6 @@
     norms = [
         push("nm", (k,), norm_own, norm_all.at[me], others[k]) for k in range(n - 1)
     ]
-    to_pair(1)
     store(g_v, outs[1])
     finish(0)
     for copy_in in c2:
@@ -649,6 +720,8 @@
         made.wait_send()
     for made in stores:
         made.wait()
+    for flag, made in guarded:
+        pl.when(flag)(made.wait_send)
     pl.when(y == 0)(hu_near.wait_send)
     pl.when(jnp.logical_and(y == 1, upper == 0))(hu_far.wait_send)
     pl.when(y == 1)(hd_near.wait_send)
@@ -716,7 +789,8 @@
     shard, width = w_conv_up.shape
     rows, features = inputs.shape
     fits = n == 8 and t == 4 and features == 2 * shard
-    aligned = shard % 8 == 0 and rows % LANES == 0 and width > LANES
+    aligned = shard % 8 == 0 and rows % LANES == 0 and width > 2 * LANES
+    aligned = aligned and width % (2 * LANES) == LANES + LANES // 2
     chosen = with_kernel if fits and aligned else with_collectives
     return chosen(inputs, w_conv_up, *rest)
 

time: 125 us -> 119 us (0.952)
  Pallas kernels: 124 us -> 118 us
    pallas_call x1, Pallas kernels: 122 us -> 116 us  [with_kernel(): pl.pallas_call(functools.partial(layer_kernel, n, t, tuple(scratch)), out...]
where the time goes in v3:
time: 119 us
  Pallas kernels  118 us (99%)
    pallas_call x1, Pallas kernels, with_kernel(): pl.pallas_call(functools.partial(layer_kernel, n, t, tuple(scratch)), out...  116 us

profile of v3, /device:TPU:0, one launch (start us, length us, event | category | flops | bytes accessed | tf_op | source)
XLA Modules:
  0.0 119.3 jit_solution(4523051316257901628)
XLA Ops:
  0.6 116.2 %layer.1 = (bf16[2,264,512]{2,1,0:T(8,128)(2,1)}, f32[264,704]{1,0:T(8,128)}, f32[704]{0:T(1024)}, f32[3,2816]{1,0:T(4,128)}, f32[2816]{0:T(1024)}) custom-call(bf16[264,704]{1,0:T(8,128)(2,1)} %bitcast.12, bf16[264,704]{1,0:T(8,128)(2,1)} %refs_1_.1, bf16[264,704]{1,0:T(8,128)(2,1)} %refs_2_.1, bf16[2,264,512]{2,1,0:T(8,128)(2,1)} %bitcast.10, ...), custom_call_target="tpu_custom_call" | custom-call | tf_op jit(solution)/shard_map/layer/pallas_call | solution.py:766
  116.9 2.3 %publish.1 = (bf16[2,264,512]{2,1,0:T(8,128)(2,1)}, f32[264,704]{1,0:T(8,128)}, f32[704]{0:T(1024)}, f32[3,2816]{1,0:T(4,128)}, f32[2816]{0:T(1024)}) custom-call(bf16[2,264,512]{2,1,0:T(8,128)(2,1)} %get-tuple-element.15.refs_0_, f32[264,704]{1,0:T(8,128)} %get-tuple-element.16.refs_1_, f32[704]{0:T(1024)} %get-tuple-element.17.refs_2_, ...), custom_call_target="tpu_custom_call" | custom-call | tf_op jit(solution)/shard_map/publish/pallas_call | solution.py:746

commit v4 on v3

--- a/solution.py
+++ b/solution.py
@@ -165,10 +165,10 @@
 def semaphores(n, t):
     shapes = dict(
         wz=(3, 3), wy=(3, 4), ez=(3, 3), ey=(3, 4), az=(4,), ax=(2, 4), ac=(4, 4), hu=(2,), hd=(2,),
-        c1=(3,), c2=(2 * t - 1,), gy=(4, 2), gz=(4, 2), pc=(8,), px=(4,), pz=(2,), nm=(n - 1,),
+        c1=(3,), c2=(2 * t - 1,), gy=(4, 2), gz=(4, 2), pc=(8,), px=(4, 2), pz=(2, 2), nm=(n - 1,),
     )
     dma = pltpu.SemaphoreType.DMA
-    local = dict(ld=dma((9,)), st=dma((6,)))
+    local = dict(ld=dma((9,)), st=dma((8,)))
     return local | {name + end: dma(s) for name, s in shapes.items() for end in ("_s", "_r")}
 
 
@@ -538,19 +538,24 @@
         b, xx, at = (1 - l, l)[bi], (1 - x, x)[xi], spot(bi, xi, half)
         pown[at] = input_grad(b, 2 * (xx * 2 + c) + half)
 
+    first_rows = -(-shard // 16) * 8
+    parts = (pl.ds(0, first_rows), pl.ds(first_rows, shard - first_rows))
+
     def to_x(bi, half):
         at, to = spot(bi, 0, half), bi * 2 + half
         pc[at].wait_recv()
-        xsend[to] = (pown[at] + crecv[at].astype(f32)).astype(b16)
-        px[to] = push("px", (to,), xsend.at[to], xrecv.at[to], x_dev)
-
-    def to_pair(half):
-        at = spot(0, 1, half)
-        pc[at].wait_recv()
-        px[half].wait_recv()
-        total = pown[at] + crecv[at].astype(f32) + xrecv[half].astype(f32)
-        psend[half] = total.astype(b16)
-        pz[half] = push("pz", (half,), psend.at[half], precv.at[half], pair)
+        for s, r in enumerate(parts):
+            xsend[to, r, :] = (pown[at, r, :] + crecv[at, r, :].astype(f32)).astype(b16)
+            px[to, s] = push("px", (to, s), xsend.at[to, r], xrecv.at[to, r], x_dev)
+
+    def to_pair(half, s):
+        at, r = spot(0, 1, half), parts[s]
+        if s == 0:
+            pc[at].wait_recv()
+        px[half, s].wait_recv()
+        total = pown[at, r, :] + crecv[at, r, :].astype(f32) + xrecv[half, r, :].astype(f32)
+        psend[half, r, :] = total.astype(b16)
+        pz[half, s] = push("pz", (half, s), psend.at[half, r], precv.at[half, r], pair)
 
     i_v, g_v, norm_v, taps_w, bias_w = (
         m[k] for k in ("i_v", "g_v", "norm_v", "taps_w", "bias_w")
@@ -565,15 +570,14 @@
     def finish(half):
         at = spot(1, 1, half)
         pc[at].wait_recv()
-        px[2 + half].wait_recv()
-        pz[half].wait_recv()
-        total = pown[at] + crecv[at].astype(f32)
-        total = total + xrecv[2 + half].astype(f32) + precv[half].astype(f32)
-        i_v[half] = total.astype(b16)
-        store(i_v.at[half], outs[0].at[half])
-
-    first_rows = -(-shard // 16) * 8
-    parts = (pl.ds(0, first_rows), pl.ds(first_rows, shard - first_rows))
+        for s, r in enumerate(parts):
+            px[2 + half, s].wait_recv()
+            pz[half, s].wait_recv()
+            total = pown[at, r, :] + crecv[at, r, :].astype(f32)
+            total = total + xrecv[2 + half, r, :].astype(f32) + precv[half, r, :].astype(f32)
+            i_v[half, r, :] = total.astype(b16)
+            store(i_v.at[half, r], outs[0].at[half, r])
+
     first_to = inner_i * zo + (1 - inner_i) * far
     first_at = 3 - 2 * inner_i
     last_at = 2 - inner_i
@@ -613,7 +617,7 @@
             to = {"fs": (zp if k % 2 else z) * 2 + y, "tp": tp}
             c2.append(push("c2", (k - 1,), m["col_sum"], place, to))
 
-    c2 = []
+    early, c2 = list(started), []
     to_across(0)
     to_twin(0, 0, 0)
     to_across(1)
@@ -625,28 +629,33 @@
     to_x(0, 1)
     to_across(2)
     to_across(3)
+    def to_other_half(k, s):
+        add_across(k, s)
+        zsend[k, parts[s], :] = gown[k, parts[s], :].astype(b16)
+        if k == 0:
+            to_line(0, s, first_to, first_at)
+        else:
+            to_line(1, s, zo, 0)
+
     own(0)
-    for s in range(2):
-        add_across(0, s)
-        zsend[0, parts[s], :] = gown[0, parts[s], :].astype(b16)
-        to_line(0, s, first_to, first_at)
+    to_other_half(0, 0)
+    to_twin(0, 1, 0)
+    to_twin(0, 1, 1)
+    keep(0, 1, 0)
+    to_other_half(0, 1)
+    keep(0, 1, 1)
     own(1)
+    to_pair(0, 0)
     to_twin(1, 0, 0)
+    to_other_half(1, 0)
     to_twin(1, 0, 1)
+    to_pair(0, 1)
     keep(1, 0, 0)
     to_x(1, 0)
-    for s in range(2):
-        add_across(1, s)
-        zsend[1, parts[s], :] = gown[1, parts[s], :].astype(b16)
-        to_line(1, s, zo, 0)
+    to_other_half(1, 1)
     keep(1, 0, 1)
     to_x(1, 1)
     own(2)
-    to_twin(0, 1, 0)
-    to_twin(0, 1, 1)
-    keep(0, 1, 0)
-    keep(0, 1, 1)
-    to_pair(0)
     for s in range(2):
         add_across(2, s)
 
@@ -660,7 +669,8 @@
             zsend[2, at, :] = (gown[2, at, :] + zrecv[1, at, :].astype(f32)).astype(b16)
 
         to_line(2, s, zp, last_at)
-    to_pair(1)
+    to_pair(1, 0)
+    to_pair(1, 1)
     own(3)
     for half in range(2):
         to_twin(1, 1, half)
@@ -694,6 +704,10 @@
         push("nm", (k,), norm_own, norm_all.at[me], others[k]) for k in range(n - 1)
     ]
     store(g_v, outs[1])
+    for made in early:
+        made.wait_send()
+    for flag, made in guarded:
+        pl.when(flag)(made.wait_send)
     finish(0)
     for copy_in in c2:
         copy_in.wait_recv()
@@ -716,12 +730,10 @@
     norm_v[:ca] = total[0]
     norm_v[ca:] = total[1, :cb]
     store(norm_v, outs[2])
-    for made in started:
+    for made in started[len(early) :]:
         made.wait_send()
     for made in stores:
         made.wait()
-    for flag, made in guarded:
-        pl.when(flag)(made.wait_send)
     pl.when(y == 0)(hu_near.wait_send)
     pl.when(jnp.logical_and(y == 1, upper == 0))(hu_far.wait_send)
     pl.when(y == 1)(hd_near.wait_send)

time: 119 us -> 117 us (0.983)
  Pallas kernels: 118 us -> 116 us
    pallas_call x1, Pallas kernels: 116 us -> 114 us  [with_kernel(): pl.pallas_call(functools.partial(layer_kernel, n, t, tuple(scratch)), out...]
where the time goes in v4:
time: 117 us
  Pallas kernels  116 us (99%)
    pallas_call x1, Pallas kernels, with_kernel(): pl.pallas_call(functools.partial(layer_kernel, n, t, tuple(scratch)), out...  114 us

profile of v4, /device:TPU:0, one launch (start us, length us, event | category | flops | bytes accessed | tf_op | source)
XLA Modules:
  0.0 116.9 jit_solution(8089610005437262792)
XLA Ops:
  0.6 113.8 %layer.1 = (bf16[2,264,512]{2,1,0:T(8,128)(2,1)}, f32[264,704]{1,0:T(8,128)}, f32[704]{0:T(1024)}, f32[3,2816]{1,0:T(4,128)}, f32[2816]{0:T(1024)}) custom-call(bf16[264,704]{1,0:T(8,128)(2,1)} %bitcast.12, bf16[264,704]{1,0:T(8,128)(2,1)} %refs_1_.1, bf16[264,704]{1,0:T(8,128)(2,1)} %refs_2_.1, bf16[2,264,512]{2,1,0:T(8,128)(2,1)} %bitcast.10, ...), custom_call_target="tpu_custom_call" | custom-call | tf_op jit(solution)/shard_map/layer/pallas_call | solution.py:778
  114.4 2.3 %publish.1 = (bf16[2,264,512]{2,1,0:T(8,128)(2,1)}, f32[264,704]{1,0:T(8,128)}, f32[704]{0:T(1024)}, f32[3,2816]{1,0:T(4,128)}, f32[2816]{0:T(1024)}) custom-call(bf16[2,264,512]{2,1,0:T(8,128)(2,1)} %get-tuple-element.15.refs_0_, f32[264,704]{1,0:T(8,128)} %get-tuple-element.16.refs_1_, f32[704]{0:T(1024)} %get-tuple-element.17.refs_2_, ...), custom_call_target="tpu_custom_call" | custom-call | tf_op jit(solution)/shard_map/publish/pallas_call | solution.py:758

commit v5 on v4

--- a/solution.py
+++ b/solution.py
@@ -620,13 +620,13 @@
     early, c2 = list(started), []
     to_across(0)
     to_twin(0, 0, 0)
+    keep(0, 0, 0)
+    to_twin(0, 0, 1)
+    to_x(0, 0)
     to_across(1)
-    to_twin(0, 0, 1)
-    keep(0, 0, 0)
-    send_columns()
-    to_x(0, 0)
     keep(0, 0, 1)
     to_x(0, 1)
+    send_columns()
     to_across(2)
     to_across(3)
     def to_other_half(k, s):

time: 117 us -> 117 us (level)
  no operation moved by 1% of the time
where the time goes in v5:
time: 117 us
  Pallas kernels  116 us (99%)
    pallas_call x1, Pallas kernels, with_kernel(): pl.pallas_call(functools.partial(layer_kernel, n, t, tuple(scratch)), out...  114 us

profile of v5, /device:TPU:0, one launch (start us, length us, event | category | flops | bytes accessed | tf_op | source)
XLA Modules:
  0.0 117.2 jit_solution(10918802820433399388)
XLA Ops:
  0.6 114.1 %layer.1 = (bf16[2,264,512]{2,1,0:T(8,128)(2,1)}, f32[264,704]{1,0:T(8,128)}, f32[704]{0:T(1024)}, f32[3,2816]{1,0:T(4,128)}, f32[2816]{0:T(1024)}) custom-call(bf16[264,704]{1,0:T(8,128)(2,1)} %bitcast.12, bf16[264,704]{1,0:T(8,128)(2,1)} %refs_1_.1, bf16[264,704]{1,0:T(8,128)(2,1)} %refs_2_.1, bf16[2,264,512]{2,1,0:T(8,128)(2,1)} %bitcast.10, ...), custom_call_target="tpu_custom_call" | custom-call | tf_op jit(solution)/shard_map/layer/pallas_call | solution.py:778
  114.7 2.3 %publish.1 = (bf16[2,264,512]{2,1,0:T(8,128)(2,1)}, f32[264,704]{1,0:T(8,128)}, f32[704]{0:T(1024)}, f32[3,2816]{1,0:T(4,128)}, f32[2816]{0:T(1024)}) custom-call(bf16[2,264,512]{2,1,0:T(8,128)(2,1)} %get-tuple-element.15.refs_0_, f32[264,704]{1,0:T(8,128)} %get-tuple-element.16.refs_1_, f32[704]{0:T(1024)} %get-tuple-element.17.refs_2_, ...), custom_call_target="tpu_custom_call" | custom-call | tf_op jit(solution)/shard_map/publish/pallas_call | solution.py:758
